TPU v7x, 32 devices: a whole 2x2x4 slice. The times are simulated.
32 devices in a mesh: fs: 8 (over z, x), tp: 4 (over y, core).
Axes of the slice: x: 2, y: 2, z: 4, core: 2. Of those that a mesh axis runs over, the one named last changes fastest.
Arguments:
- inputs: bfloat16 [1024, 2048], P('fs', 'tp'), may hold values from -6 to 6
- query_grad: bfloat16 [1024, 1024], P('fs', 'tp'), may hold values from -6 to 6
- forget_grad: bfloat16 [1024, 1024], P('fs', 'tp'), may hold values from -6 to 6
- forget_pre: bfloat16 [1024, 1024], P('fs', 'tp'), may hold values from -8 to 8
- lower_bound: float32 [1024], P('tp'), may hold values from 0.1 to 0.9
- query_weight: float32 [2048, 1024], P('fs', 'tp'), may hold values from -0.125 to 0.125
- forget_weight: float32 [2048, 1024], P('fs', 'tp'), may hold values from -0.125 to 0.125
- query_moment: float32 [2048, 1024], P('fs', 'tp'), may hold values from -6 to 6
- forget_moment: float32 [2048, 1024], P('fs', 'tp'), may hold values from -6 to 6
- query_rows: float32 [2048, 2048], P('fs'), may hold values from -0.6 to 0.6
- forget_rows: float32 [2048, 2048], P('fs'), may hold values from -0.6 to 0.6
- query_cols: float32 [8, 128, 128], P('tp'), may hold values from -0.6 to 0.6
- forget_cols: float32 [8, 128, 128], P('tp'), may hold values from -0.6 to 0.6
- query_row_root: bfloat16 [2048, 2048], P('fs'), may hold values from -2 to 2, as said below
- forget_row_root: bfloat16 [2048, 2048], P('fs'), may hold values from -2 to 2, as said below
- query_col_root: bfloat16 [8, 128, 128], P('tp'), may hold values from -2 to 2, as said below
- forget_col_root: bfloat16 [8, 128, 128], P('tp'), may hold values from -2 to 2, as said below
Outputs:
- query_master: float32 [2048, 1024], P('fs', 'tp')
- forget_master: float32 [2048, 1024], P('fs', 'tp')
- query_copy: bfloat16 [2048, 1024], P('fs', 'tp')
- forget_copy: bfloat16 [2048, 1024], P('fs', 'tp')
- query_step: float32 [2048, 1024], P('fs', 'tp')
- forget_step: float32 [2048, 1024], P('fs', 'tp')
- query_moment_next: float32 [2048, 1024], P('fs', 'tp')
- forget_moment_next: float32 [2048, 1024], P('fs', 'tp')
- query_rows_next: float32 [2048, 2048], P('fs')
- forget_rows_next: float32 [2048, 2048], P('fs')
- query_cols_next: float32 [8, 128, 128], P('tp')
- forget_cols_next: float32 [8, 128, 128], P('tp')
Inputs may be any that keep to these rules, and one draw needn't show every extreme that they name: `query_row_root`: diagonal entries 0.5 to 1.5, the others of order 2048 ** -0.5. `forget_row_root`: diagonal entries 0.5 to 1.5, the others of order 2048 ** -0.5. `query_col_root`: diagonal entries 0.5 to 1.5, the others of order 128 ** -0.5. `forget_col_root`: diagonal entries 0.5 to 1.5, the others of order 128 ** -0.5.
All inputs are finite; a program needn't handle non-finite values.
Results may differ from a plain program's by a relative error of at most 0.005.
Values may be sent and summed in bfloat16 or wider, within the bound.
A program may use at most 64 MiB of HBM per device.

v0:
```python
import functools

import jax
import jax.numpy as jnp
from jax import lax
from jax.experimental import pallas as pl
from jax.experimental.pallas import tpu as pltpu
from jax.sharding import PartitionSpec as P

D = 2048
HW = 1024
HEAD = 128


stat_decay = 0.9
moment_decay = 0.9
learn_rate = 0.02
highest = lax.Precision.HIGHEST
MESH = pl.DeviceIdType.MESH


def fold_one(carry_state, shard_piece, offset, root_mine, grad_mine):
    left_sum, outer_rows, column_total = carry_state
    row_count, col_width = shard_piece.shape
    left_sum = left_sum + jnp.dot(root_mine, shard_piece, precision=highest)
    outer_piece = lax.dot_general(
        grad_mine, shard_piece, (((1,), (1,)), ((), ())), precision=highest
    )
    outer_rows = lax.dynamic_update_slice_in_dim(outer_rows, outer_piece, offset, 1)
    by_head = shard_piece.reshape(row_count, col_width // HEAD, HEAD)
    column_total = column_total + jnp.einsum("rhi,rhj->hij", by_head, by_head, precision=highest)
    return (left_sum, outer_rows, column_total)


def finish(weight, moment, rows, cols, col_root, left_sum, outer_rows, column_total, square):
    norm_scale = jnp.sqrt(D * HW / (square + 1.0))
    scale_twice = norm_scale * norm_scale
    rows_next = stat_decay * rows + (1.0 - stat_decay) / HW * scale_twice * outer_rows
    cols_next = stat_decay * cols + (1.0 - stat_decay) / D * scale_twice * column_total
    shard_rows, col_width = left_sum.shape
    shaped = left_sum.reshape(shard_rows, col_width // HEAD, HEAD)
    precond = norm_scale * jnp.einsum(
        "rhi,hij->rhj", shaped, col_root.astype(jnp.float32), precision=highest
    ).reshape(shard_rows, col_width)
    moment_next = moment_decay * moment + (1.0 - moment_decay) * precond
    update_step = moment_decay * moment_next + (1.0 - moment_decay) * precond
    master = weight - learn_rate * update_step
    return (master, master.astype(jnp.bfloat16), update_step, moment_next, rows_next, cols_next)


def reduce_plan(
    inputs,
    query_grad,
    forget_grad,
    forget_pre,
    lower_bound,
    query_weight,
    forget_weight,
    query_moment,
    forget_moment,
    query_rows,
    forget_rows,
    query_cols,
    forget_cols,
    query_row_root,
    forget_row_root,
    query_col_root,
    forget_col_root,
):
    sigma_gate = jax.nn.sigmoid(forget_pre.astype(jnp.float32))
    forget_cot = (
        forget_grad.astype(jnp.float32) * (1.0 - lower_bound) * sigma_gate * (1.0 - sigma_gate)
    ).astype(jnp.bfloat16)
    gathered = lax.all_gather(inputs, "tp", axis=1, tiled=True)
    shard_rows, col_width = query_weight.shape
    heads_here = col_width // HEAD
    row_roots = (query_row_root.astype(jnp.float32), forget_row_root.astype(jnp.float32))
    empty = (
        jnp.zeros((shard_rows, col_width), jnp.float32),
        jnp.zeros((shard_rows, D), jnp.float32),
        jnp.zeros((heads_here, HEAD, HEAD), jnp.float32),
    )
    joined = jnp.concatenate([query_grad, forget_cot], axis=1)
    summed = lax.psum_scatter(
        lax.dot_general(
            gathered, joined, (((0,), (0,)), ((), ())), preferred_element_type=jnp.float32
        ),
        "fs",
        scatter_dimension=0,
        tiled=True,
    )
    gradients = (summed[:, :col_width], summed[:, col_width:])
    offset = jnp.int32(0)
    results = (
        fold_one(
            empty,
            lax.all_gather(gradients[0].astype(jnp.bfloat16), "fs", axis=0, tiled=True).astype(
                jnp.float32
            ),
            offset,
            row_roots[0],
            gradients[0],
        ),
        fold_one(
            empty,
            lax.all_gather(gradients[1].astype(jnp.bfloat16), "fs", axis=0, tiled=True).astype(
                jnp.float32
            ),
            offset,
            row_roots[1],
            gradients[1],
        ),
    )
    query_trace = jnp.sum(jnp.diagonal(results[0][2], axis1=1, axis2=2))
    forget_trace = jnp.sum(jnp.diagonal(results[1][2], axis1=1, axis2=2))
    query_outer, forget_outer, query_square, forget_square = (
        lax.psum(results[0][1].astype(jnp.bfloat16), "tp").astype(jnp.float32),
        lax.psum(results[1][1].astype(jnp.bfloat16), "tp").astype(jnp.float32),
        lax.psum(query_trace.astype(jnp.bfloat16), "tp").astype(jnp.float32),
        lax.psum(forget_trace.astype(jnp.bfloat16), "tp").astype(jnp.float32),
    )
    query_out = finish(
        query_weight,
        query_moment,
        query_rows,
        query_cols,
        query_col_root,
        results[0][0],
        query_outer,
        results[0][2],
        query_square,
    )
    forget_out = finish(
        forget_weight,
        forget_moment,
        forget_rows,
        forget_cols,
        forget_col_root,
        results[1][0],
        forget_outer,
        results[1][2],
        forget_square,
    )
    return (
        query_out[0],
        forget_out[0],
        query_out[1],
        forget_out[1],
        query_out[2],
        forget_out[2],
        query_out[3],
        forget_out[3],
        query_out[4],
        forget_out[4],
        query_out[5],
        forget_out[5],
    )


def to_bf16(value):
    return value.astype(jnp.bfloat16)


def wide_dot(left, right, dims):
    return lax.dot_general(left, right, (dims, ((), ())), preferred_element_type=jnp.float32)


def relay_kernel(
    x_ref, g_ref, rq_hbm, rf_hbm, cq_ref, cf_ref,
    s_ref, pq_ref, pf_ref, kq_ref, kf_ref,
    xs, gs, xt, acc, other, grad, owned, left, norms, roots, own_sem, send_sem, recv_sem, swap_sem,
):
    shards = xs.shape[0]
    depth = shards // 2
    block, span = x_ref.shape
    fs = lax.axis_index("fs")
    tp = lax.axis_index("tp")
    z, px = lax.div(fs, 2), lax.rem(fs, 2)
    py, pc = lax.div(tp, 2), lax.rem(tp, 2)
    fs_other = fs + 1 - 2 * px
    tp_other = tp + 2 - 4 * py
    beside = {
        "up": (fs + 2, tp),
        "down": (fs - 2, tp),
        "x": (fs_other, tp),
        "y": (fs, tp_other),
        "core": (fs, tp + 1 - 2 * pc),
    }
    has_up = z < depth - 1
    has_down = z > 0

    def guarded(cond, action):
        if cond is None:
            action()
        else:
            pl.when(cond)(action)

    barrier = pltpu.get_barrier_semaphore()

    def greet(name):
        pl.semaphore_signal(barrier, inc=1, device_id=beside[name], device_id_type=MESH)

    for name in ("x", "y", "core"):
        greet(name)
    guarded(has_up, lambda: greet("up"))
    guarded(has_down, lambda: greet("down"))
    pl.semaphore_wait(
        barrier, 3 + jnp.where(has_up, 1, 0) + jnp.where(has_down, 1, 0)
    )

    slots = (xs, gs)
    pending = []

    def place(kind, slot, half):
        if kind == 1 and half is not None:
            return slots[kind].at[slot[0], slot[1], half]
        return slots[kind].at[slot[0], slot[1]]

    def copy_of(kind, src, slot, name, number, half=None):
        return pltpu.make_async_remote_copy(
            src_ref=src,
            dst_ref=place(kind, slot, half),
            send_sem=send_sem.at[number],
            recv_sem=recv_sem.at[kind, slot[0], slot[1]],
            device_id=beside[name],
            device_id_type=MESH,
        )

    def send(kind, src, slot, name, cond=None):
        number = len(pending)
        half = 1 - pc if name == "core" else None
        if kind == 1 and half is not None:
            src = src.at[half]
        build = functools.partial(copy_of, kind, src, slot, name, number, half)
        guarded(cond, lambda: build().start())
        pending.append((cond, build))

    def arrive(kind, slot, cond=None, half=None):
        here = place(kind, slot, half)
        guarded(cond, lambda: copy_of(kind, here, slot, "core", 0, half).wait_recv())

    def forward(kind, slot, names, cond=None):
        for name in names:
            send(kind, slots[kind].at[slot[0], slot[1]], slot, name, cond)

    own = (fs, tp)
    orders = (("x", "y"), ("y", "x"))
    sources = (x_ref, g_ref)

    def crossed(kind, layer):
        if kind == 0:
            return (2 * layer + 1 - px, tp)
        return (2 * layer + px, tp_other)

    def lasts(kind, layer):
        if kind == 0:
            return ((2 * layer + px, tp_other), (2 * layer + 1 - px, tp_other))
        return ((2 * layer + 1 - px, tp), (2 * layer + 1 - px, tp_other))

    keep = [
        pltpu.make_async_copy(sources[kind], slots[kind].at[fs, tp], own_sem.at[kind])
        for kind in range(2)
    ]
    loads = [
        pltpu.make_async_copy(source, roots.at[which], own_sem.at[2 + which])
        for which, source in enumerate((rq_hbm, rf_hbm))
    ]
    for kind in range(2):
        send(kind, sources[kind], own, "up", has_up)
        send(kind, sources[kind], own, "down", has_down)
    for kind in range(2):
        send(kind, sources[kind], own, orders[kind][0])
    for kind in range(2):
        send(kind, sources[kind], own, orders[kind][1])
        send(kind, sources[kind], own, "core")
        keep[kind].start()
        loads[kind].start()

    def finals(stage):
        for layer, cond in stage:
            for kind in range(2):
                for slot in lasts(kind, layer):
                    arrive(kind, slot, cond)
                    forward(kind, slot, ("core",), cond)

    width = gs.shape[4]
    parts = gs.shape[1]
    chunk = s_ref.shape[1]
    steps = acc.shape[0] // chunk
    own_lanes = pl.ds(pl.multiple_of(tp * width, width), width)
    low = jnp.minimum(z, depth - 1 - z)

    def layer_of(turn):
        if turn == 0:
            return z
        near = z - (turn + 1) // 2 if turn % 2 == 1 else z + turn // 2
        far = jnp.where(2 * z < depth, turn, depth - 1 - turn)
        return jnp.where(turn <= 2 * low, near, far)

    def multiply(turn):
        layer = layer_of(turn)
        for across in range(2):
            for part in range(2):
                slot = (2 * layer + across, 2 * part + 1 - pc)
                for kind in range(2):
                    arrive(kind, slot, half=pc)
        for across in range(2):
            for part in range(parts):
                block_t = xs[2 * layer + across, part].T
                xt[part * span : (part + 1) * span, across * block : (across + 1) * block] = block_t
        first, final = turn == 0, turn == depth - 1
        both = pl.ds(2 * layer, 2)

        def step_body(step, total):
            rows = pl.ds(pl.multiple_of(step * chunk, chunk), chunk)
            for part in range(parts):
                cot = gs[both, part, pc].reshape(2 * block, width)
                piece = wide_dot(xt[rows, :], cot, ((1,), (0,)))
                lanes = slice(part * width, (part + 1) * width)
                if not first:
                    piece = piece + acc[rows, lanes]
                if final:
                    grad[rows, lanes] = to_bf16(piece)
                    total = total + jnp.sum(piece * piece, axis=0, keepdims=True)
                else:
                    acc[rows, lanes] = piece
            cot = gs[both, tp, 1 - pc].reshape(2 * block, width)
            piece = wide_dot(xt[rows, :], cot, ((1,), (0,)))
            if not first:
                piece = piece + other[rows, :]
            if final:
                owned[1 - pc, rows, :] = to_bf16(piece)
            else:
                other[rows, :] = piece
            return total

        return lax.fori_loop(0, steps, step_body, jnp.zeros((1, width), jnp.float32))

    def layers_at(distance):
        if distance == 0:
            return ((z, None),)
        return (
            (z - distance, z >= distance),
            (z + distance, z + distance < depth),
        )

    def along(distance):
        for onward, (layer, cond), more in zip(
            ("up", "down"), layers_at(distance), (has_up, has_down)
        ):
            for kind in range(2):
                slot = (2 * layer + px, tp)
                arrive(kind, slot, cond)
                if distance < depth - 1:
                    forward(kind, slot, (onward,), jnp.logical_and(cond, more))
                forward(kind, slot, orders[kind] + ("core",), cond)

    def across_pair(distance):
        for layer, cond in layers_at(distance):
            for kind in range(2):
                slot = crossed(kind, layer)
                arrive(kind, slot, cond)
                forward(kind, slot, (orders[kind][1], "core"), cond)

    for distance in range(1, depth):
        along(distance)
        if distance < depth - 1:
            across_pair(distance - 1)
    finals(layers_at(0))
    for kind in range(2):
        keep[kind].wait()
    multiply(0)
    across_pair(depth - 2)
    across_pair(depth - 1)
    for distance in range(1, depth - 1):
        finals(layers_at(distance))
        multiply(distance)
    finals(layers_at(depth - 1))
    total = multiply(depth - 1)

    tp_core = (fs, tp + 1 - 2 * pc)
    square = jnp.sum(total, axis=1, keepdims=True)
    norms[0] = jnp.broadcast_to(square, norms.shape[1:])
    swap_norm = pltpu.make_async_remote_copy(
        src_ref=norms.at[0], dst_ref=norms.at[1],
        send_sem=swap_sem.at[0], recv_sem=swap_sem.at[1],
        device_id=tp_core, device_id_type=MESH,
    )
    swap_rows = pltpu.make_async_remote_copy(
        src_ref=s_ref.at[pc], dst_ref=s_ref.at[pc],
        send_sem=swap_sem.at[2], recv_sem=swap_sem.at[3],
        device_id=tp_core, device_id_type=MESH,
    )
    take_rows = pltpu.make_async_remote_copy(
        src_ref=s_ref.at[1 - pc], dst_ref=s_ref.at[1 - pc],
        send_sem=swap_sem.at[2], recv_sem=swap_sem.at[3],
        device_id=tp_core, device_id_type=MESH,
    )
    size = float(grad.shape[0] * grad.shape[1])
    outer_scale = (1.0 - stat_decay) / grad.shape[1] * (size / (square + 1.0))
    mine = pl.ds(pl.multiple_of(fs * chunk, chunk), chunk)

    @pl.loop(0, steps)
    def _(step):
        rows = pl.ds(pl.multiple_of(step * chunk, chunk), chunk)
        outer = wide_dot(grad[mine, :], grad[rows, :], ((1,), (1,)))
        s_ref[pc, :, rows] = to_bf16(outer * outer_scale)
        owned[pc, rows, :] = grad[rows, own_lanes]

    swap_norm.start()
    heads = width // HEAD
    left[...] = jnp.zeros_like(left)
    kq_ref[...] = jnp.zeros_like(kq_ref)
    kf_ref[...] = jnp.zeros_like(kf_ref)
    swap_rows.start()
    for load in loads:
        load.wait()

    @pl.loop(0, steps)
    def _(step):
        rows = pl.ds(pl.multiple_of(step * chunk, chunk), chunk)
        for which, (root, col_ref) in enumerate(((roots.at[0], kq_ref), (roots.at[1], kf_ref))):
            part = owned[which, rows, :]
            left[which] += wide_dot(root[:, rows], part, ((1,), (0,)))
            for head in range(heads):
                piece = part[:, head * HEAD : (head + 1) * HEAD]
                col_ref[head] += wide_dot(piece, piece, ((0,), (0,)))

    swap_norm.wait()
    mine_sum, their_sum = norms[0, 0:1, 0:1], norms[1, 0:1, 0:1]
    sums = (
        jnp.where(pc == 0, mine_sum, their_sum),
        jnp.where(pc == 0, their_sum, mine_sum),
    )
    for which, (col_root, pre_ref, col_ref) in enumerate(
        ((cq_ref, pq_ref, kq_ref), (cf_ref, pf_ref, kf_ref))
    ):
        scale_twice = size / (sums[which] + 1.0)
        norm_scale = jnp.sqrt(scale_twice)
        for head in range(heads):
            lanes = slice(head * HEAD, (head + 1) * HEAD)
            col_ref[head] = col_ref[head] * ((1.0 - stat_decay) / grad.shape[0] * scale_twice)
            pre_ref[:, lanes] = norm_scale * wide_dot(
                to_bf16(left[which, :, lanes]), col_root[head], ((1,), (0,))
            )
    swap_rows.wait_send()
    take_rows.wait_recv()

    for cond, build in pending:
        guarded(cond, lambda build=build: build().wait_send())


def relayed_products(x, cots, query_root, forget_root, query_col_root, forget_col_root):
    shards, parts = lax.axis_size("fs"), lax.axis_size("tp")
    block, span = x.shape
    width = cots.shape[2]
    chunk, features = query_root.shape
    depth = shards // 2
    sends = 2 * (5 + 8 * (depth - 1) + 2 * (2 * depth - 1) + 2 * (2 * depth - 1))
    f32 = jnp.float32
    heads = query_col_root.shape
    vmem = pl.BlockSpec(memory_space=pltpu.VMEM)
    hbm = pl.BlockSpec(memory_space=pltpu.HBM)
    return pl.pallas_call(
        relay_kernel,
        out_shape=[
            jax.ShapeDtypeStruct((2, chunk, features), jnp.bfloat16),
            jax.ShapeDtypeStruct((chunk, width), f32),
            jax.ShapeDtypeStruct((chunk, width), f32),
            jax.ShapeDtypeStruct(heads, f32),
            jax.ShapeDtypeStruct(heads, f32),
        ],
        in_specs=[vmem, vmem, hbm, hbm, vmem, vmem],
        out_specs=[vmem] * 5,
        scratch_shapes=[
            pltpu.VMEM((shards, parts, block, span), jnp.bfloat16),
            pltpu.VMEM((shards, parts, 2, block, width), jnp.bfloat16),
            pltpu.VMEM((features, 2 * block), jnp.bfloat16),
            pltpu.VMEM((features, parts * width), f32),
            pltpu.VMEM((features, width), f32),
            pltpu.VMEM((features, parts * width), jnp.bfloat16),
            pltpu.VMEM((2, features, width), jnp.bfloat16),
            pltpu.VMEM((2, chunk, width), f32),
            pltpu.VMEM((2, 8, 128), f32),
            pltpu.VMEM((2, chunk, features), jnp.bfloat16),
            pltpu.SemaphoreType.DMA((4,)),
            pltpu.SemaphoreType.DMA((sends,)),
            pltpu.SemaphoreType.DMA((2, shards, parts)),
            pltpu.SemaphoreType.DMA((4,)),
        ],
        compiler_params=pltpu.CompilerParams(
            collective_id=0, has_side_effects=True, vmem_limit_bytes=61 * 1024 * 1024
        ),
    )(x, cots, query_root, forget_root, query_col_root, forget_col_root)


def pack_kernel(query_ref, forget_ref, pre_ref, bound_ref, out_ref):
    out_ref[0] = query_ref[...]
    sigma_gate = jax.nn.sigmoid(pre_ref[...].astype(jnp.float32))
    out_ref[1] = to_bf16(
        forget_ref[...].astype(jnp.float32)
        * (1.0 - bound_ref[...])
        * sigma_gate
        * (1.0 - sigma_gate)
    )


def packed_cotangents(query_grad, forget_grad, forget_pre, lower_bound):
    vmem = pl.BlockSpec(memory_space=pltpu.VMEM)
    return pl.pallas_call(
        pack_kernel,
        out_shape=jax.ShapeDtypeStruct((2,) + query_grad.shape, jnp.bfloat16),
        in_specs=[vmem] * 4,
        out_specs=vmem,
        compiler_params=pltpu.CompilerParams(vmem_limit_bytes=61 * 1024 * 1024),
    )(query_grad, forget_grad, forget_pre, lower_bound.reshape(1, -1))


def finish_kernel(outer_ref, *refs):
    pres, columns, weights, moments, rows, cols = (refs[2 * k : 2 * k + 2] for k in range(6))
    outs = refs[12:]
    for which in range(2):
        master_ref, copy_ref, step_ref, moment_ref, rows_ref, cols_ref = outs[which::2]
        precond = pres[which][...]
        moment_next = moment_decay * moments[which][...] + (1.0 - moment_decay) * precond
        update_step = moment_decay * moment_next + (1.0 - moment_decay) * precond
        master = weights[which][...] - learn_rate * update_step
        master_ref[...] = master
        copy_ref[...] = to_bf16(master)
        step_ref[...] = update_step
        moment_ref[...] = moment_next
        rows_ref[...] = stat_decay * rows[which][...] + outer_ref[which].astype(jnp.float32)
        cols_ref[...] = stat_decay * cols[which][...] + columns[which][...]


def finished(outers, pres, columns, weights, moments, rows, cols):
    f32, bf16 = jnp.float32, jnp.bfloat16
    chunk, width = weights[0].shape
    features = rows[0].shape[1]
    heads = cols[0].shape
    steps = 2
    tile = chunk // steps
    narrow = pl.BlockSpec((tile, width), lambda i: (i, 0))
    wide = pl.BlockSpec((tile, features), lambda i: (i, 0))
    head = pl.BlockSpec((heads[0], heads[1] // steps, heads[2]), lambda i: (0, i, 0))
    both = pl.BlockSpec((2, tile, features), lambda i: (0, i, 0))
    flat = lambda kind: [jax.ShapeDtypeStruct((chunk, width), kind)] * 2
    return pl.pallas_call(
        finish_kernel,
        grid=(steps,),
        out_shape=flat(f32)
        + flat(bf16)
        + flat(f32)
        + flat(f32)
        + [jax.ShapeDtypeStruct((chunk, features), f32)] * 2
        + [jax.ShapeDtypeStruct(heads, f32)] * 2,
        in_specs=[both] + [narrow] * 2 + [head] * 2 + [narrow] * 4 + [wide] * 2 + [head] * 2,
        out_specs=[narrow] * 8 + [wide] * 2 + [head] * 2,
        compiler_params=pltpu.CompilerParams(vmem_limit_bytes=61 * 1024 * 1024),
    )(outers, *pres, *columns, *weights, *moments, *rows, *cols)


def gather_plan(
    inputs,
    query_grad,
    forget_grad,
    forget_pre,
    lower_bound,
    query_weight,
    forget_weight,
    query_moment,
    forget_moment,
    query_rows,
    forget_rows,
    query_cols,
    forget_cols,
    query_row_root,
    forget_row_root,
    query_col_root,
    forget_col_root,
):
    outers, query_pre, forget_pre_out, query_column, forget_column = relayed_products(
        inputs,
        packed_cotangents(query_grad, forget_grad, forget_pre, lower_bound),
        query_row_root,
        forget_row_root,
        query_col_root,
        forget_col_root,
    )
    return tuple(
        finished(
            outers,
            (query_pre, forget_pre_out),
            (query_column, forget_column),
            (query_weight, forget_weight),
            (query_moment, forget_moment),
            (query_rows, forget_rows),
            (query_cols, forget_cols),
        )
    )


def on_device(*args):
    token_count = args[0].shape[0] * lax.axis_size("fs")
    feature_count = args[0].shape[1] * lax.axis_size("tp")
    paired = lax.axis_size("fs") % 2 == 0 and lax.axis_size("tp") == 4
    if paired and token_count <= feature_count:
        return gather_plan(*args)
    return reduce_plan(*args)


def solution(mesh):
    in_specs = (
        P("fs", "tp"),
        P("fs", "tp"),
        P("fs", "tp"),
        P("fs", "tp"),
        P("tp"),
        P("fs", "tp"),
        P("fs", "tp"),
        P("fs", "tp"),
        P("fs", "tp"),
        P("fs", None),
        P("fs", None),
        P("tp", None, None),
        P("tp", None, None),
        P("fs", None),
        P("fs", None),
        P("tp", None, None),
        P("tp", None, None),
    )
    out_specs = (
        P("fs", "tp"),
        P("fs", "tp"),
        P("fs", "tp"),
        P("fs", "tp"),
        P("fs", "tp"),
        P("fs", "tp"),
        P("fs", "tp"),
        P("fs", "tp"),
        P("fs", None),
        P("fs", None),
        P("tp", None, None),
        P("tp", None, None),
    )
    return jax.shard_map(
        on_device, mesh=mesh, in_specs=in_specs, out_specs=out_specs, check_vma=False
    )
```

profile of v0, /device:TPU:0, one launch (start us, length us, event | category | flops | bytes accessed | tf_op | source)
XLA Modules:
  0.0 65.9 jit_solution(7214577012157983288)
XLA Ops:
  0.6 1.6 %shard_map.256.g_ref = bf16[2,128,256]{2,1,0:T(8,128)(2,1)} custom-call(bf16[128,256]{1,0:T(8,128)(2,1)} %query_ref.1, bf16[128,256]{1,0:T(8,128)(2,1)} %forget_ref.1, bf16[128,256]{1,0:T(8,128)(2,1)} %pre_ref.1, f32[1,256]{1,0:T(1,128)} %bitcast.1), custom_call_target="tpu_custom_call" | custom-call | tf_op jit(solution)/shard_map/pallas_call | solution.py:510
  2.3 58.1 %shard_map.257 = (bf16[2,256,2048]{2,1,0:T(8,128)(2,1)}, f32[256,256]{1,0:T(8,128)}, f32[256,256]{1,0:T(8,128)}, f32[2,128,128]{2,1,0:T(8,128)}, f32[2,128,128]{2,1,0:T(8,128)}) custom-call(bf16[128,512]{1,0:T(8,128)(2,1)} %x_ref.1, bf16[2,128,256]{2,1,0:T(8,128)(2,1)} %shard_map.256.g_ref, bf16[256,2048]{1,0:T(8,128)(2,1)} %rq_hbm.1, ...), custom_call_target="tpu_custom_call" | custom-call | tf_op jit(solution)/shard_map/pallas_call | solution.py:464
  60.4 5.5 %shard_map.258 = (f32[256,256]{1,0:T(8,128)}, f32[256,256]{1,0:T(8,128)}, bf16[256,256]{1,0:T(8,128)(2,1)}, bf16[256,256]{1,0:T(8,128)(2,1)}, f32[256,256]{1,0:T...) custom-call(bf16[2,256,2048]{2,1,0:T(8,128)(2,1)} %get-tuple-element, ...), custom_call_target="tpu_custom_call" | custom-call | tf_op jit(solution)/shard_map/pallas_call | solution.py:548
where the time goes:
time: 66.3 us; the launch traced here: 65.9 us
  Pallas kernels  65.3 us (98%)
    pallas_call x1, Pallas kernels, relayed_products(): pl.pallas_call(relay_kernel, out_shape=[jax.ShapeDtypeStruct((2, chunk, f...  58.1 us
    pallas_call x1, Pallas kernels, finished(): pl.pallas_call(finish_kernel, grid=(steps,), out_shape=flat(f32) + flat(b...  5.55 us
    pallas_call x1, Pallas kernels, packed_cotangents(): pl.pallas_call(pack_kernel, out_shape=jax.ShapeDtypeStruct((2,) + query_g...  1.61 us

commit v1 on v0

v1 whole, which is shorter than its diff:
```python
import functools

import jax
import jax.numpy as jnp
from jax import lax
from jax.experimental import pallas as pl
from jax.experimental.pallas import tpu as pltpu
from jax.sharding import PartitionSpec as P

D = 2048
HW = 1024
HEAD = 128


stat_decay = 0.9
moment_decay = 0.9
learn_rate = 0.02
highest = lax.Precision.HIGHEST
MESH = pl.DeviceIdType.MESH


def fold_one(carry_state, shard_piece, offset, root_mine, grad_mine):
    left_sum, outer_rows, column_total = carry_state
    row_count, col_width = shard_piece.shape
    left_sum = left_sum + jnp.dot(root_mine, shard_piece, precision=highest)
    outer_piece = lax.dot_general(
        grad_mine, shard_piece, (((1,), (1,)), ((), ())), precision=highest
    )
    outer_rows = lax.dynamic_update_slice_in_dim(outer_rows, outer_piece, offset, 1)
    by_head = shard_piece.reshape(row_count, col_width // HEAD, HEAD)
    column_total = column_total + jnp.einsum("rhi,rhj->hij", by_head, by_head, precision=highest)
    return (left_sum, outer_rows, column_total)


def finish(weight, moment, rows, cols, col_root, left_sum, outer_rows, column_total, square):
    norm_scale = jnp.sqrt(D * HW / (square + 1.0))
    scale_twice = norm_scale * norm_scale
    rows_next = stat_decay * rows + (1.0 - stat_decay) / HW * scale_twice * outer_rows
    cols_next = stat_decay * cols + (1.0 - stat_decay) / D * scale_twice * column_total
    shard_rows, col_width = left_sum.shape
    shaped = left_sum.reshape(shard_rows, col_width // HEAD, HEAD)
    precond = norm_scale * jnp.einsum(
        "rhi,hij->rhj", shaped, col_root.astype(jnp.float32), precision=highest
    ).reshape(shard_rows, col_width)
    moment_next = moment_decay * moment + (1.0 - moment_decay) * precond
    update_step = moment_decay * moment_next + (1.0 - moment_decay) * precond
    master = weight - learn_rate * update_step
    return (master, master.astype(jnp.bfloat16), update_step, moment_next, rows_next, cols_next)


def reduce_plan(
    inputs,
    query_grad,
    forget_grad,
    forget_pre,
    lower_bound,
    query_weight,
    forget_weight,
    query_moment,
    forget_moment,
    query_rows,
    forget_rows,
    query_cols,
    forget_cols,
    query_row_root,
    forget_row_root,
    query_col_root,
    forget_col_root,
):
    sigma_gate = jax.nn.sigmoid(forget_pre.astype(jnp.float32))
    forget_cot = (
        forget_grad.astype(jnp.float32) * (1.0 - lower_bound) * sigma_gate * (1.0 - sigma_gate)
    ).astype(jnp.bfloat16)
    gathered = lax.all_gather(inputs, "tp", axis=1, tiled=True)
    shard_rows, col_width = query_weight.shape
    heads_here = col_width // HEAD
    row_roots = (query_row_root.astype(jnp.float32), forget_row_root.astype(jnp.float32))
    empty = (
        jnp.zeros((shard_rows, col_width), jnp.float32),
        jnp.zeros((shard_rows, D), jnp.float32),
        jnp.zeros((heads_here, HEAD, HEAD), jnp.float32),
    )
    joined = jnp.concatenate([query_grad, forget_cot], axis=1)
    summed = lax.psum_scatter(
        lax.dot_general(
            gathered, joined, (((0,), (0,)), ((), ())), preferred_element_type=jnp.float32
        ),
        "fs",
        scatter_dimension=0,
        tiled=True,
    )
    gradients = (summed[:, :col_width], summed[:, col_width:])
    offset = jnp.int32(0)
    results = (
        fold_one(
            empty,
            lax.all_gather(gradients[0].astype(jnp.bfloat16), "fs", axis=0, tiled=True).astype(
                jnp.float32
            ),
            offset,
            row_roots[0],
            gradients[0],
        ),
        fold_one(
            empty,
            lax.all_gather(gradients[1].astype(jnp.bfloat16), "fs", axis=0, tiled=True).astype(
                jnp.float32
            ),
            offset,
            row_roots[1],
            gradients[1],
        ),
    )
    query_trace = jnp.sum(jnp.diagonal(results[0][2], axis1=1, axis2=2))
    forget_trace = jnp.sum(jnp.diagonal(results[1][2], axis1=1, axis2=2))
    query_outer, forget_outer, query_square, forget_square = (
        lax.psum(results[0][1].astype(jnp.bfloat16), "tp").astype(jnp.float32),
        lax.psum(results[1][1].astype(jnp.bfloat16), "tp").astype(jnp.float32),
        lax.psum(query_trace.astype(jnp.bfloat16), "tp").astype(jnp.float32),
        lax.psum(forget_trace.astype(jnp.bfloat16), "tp").astype(jnp.float32),
    )
    query_out = finish(
        query_weight,
        query_moment,
        query_rows,
        query_cols,
        query_col_root,
        results[0][0],
        query_outer,
        results[0][2],
        query_square,
    )
    forget_out = finish(
        forget_weight,
        forget_moment,
        forget_rows,
        forget_cols,
        forget_col_root,
        results[1][0],
        forget_outer,
        results[1][2],
        forget_square,
    )
    return (
        query_out[0],
        forget_out[0],
        query_out[1],
        forget_out[1],
        query_out[2],
        forget_out[2],
        query_out[3],
        forget_out[3],
        query_out[4],
        forget_out[4],
        query_out[5],
        forget_out[5],
    )


def to_bf16(value):
    return value.astype(jnp.bfloat16)


def wide_dot(left, right, dims):
    return lax.dot_general(left, right, (dims, ((), ())), preferred_element_type=jnp.float32)


LAYERS = "ABCD"
ACROSS = {"p": {"c": "p", "p": "c", "s": "d", "d": "s"}, "s": {"c": "s", "s": "c", "p": "d", "d": "p"}}
ROUTES = {
    "Ac": ("b", "m", "p", "s"),
    "Bc": ("m", "s"),
    "Cc": ("n", "p", "s"),
    "Dc": ("n", "p", "s"),
    "Ap": ("s", "b"),
    "Cp": ("s",),
    "Dp": ("s",),
    "Ad": ("b",),
}
PROGRAM = (
    "o0", "o1", "w0Ap", "w0As", "w0Bc", "w1Ap", "w1As", "w1Bc", "w0Cc", "w0Bp", "w0Ad", "w0Bs",
    "w1Cc", "w0Cp", "w0Cs", "w1Bp", "w0Dc", "w1Ad", "TA", "w1Bs", "o2", "w1Cp", "w1Dc", "w0Bd",
    "w0Dp", "o3", "w2Ap", "w1Cs", "w0Cd", "w1Bd", "TB", "w1Dp", "w2Bc", "w0Ds", "w2Cc", "w2As",
    "w3Ap", "w1Cd", "TC", "w1Ds", "w2Bp", "w3Bc", "w2Cp", "w2Dc", "w0Dd", "w2Ad", "w3Cc", "w3As",
    "w1Dd", "TD", "w2Bs", "M20AB", "OAB", "w2Dp", "w3Bp", "w3Dc", "w2Cs", "M20C", "OC", "w3Cp",
    "w3Ad", "w2Bd", "M21AB", "w3Bs", "M30AB", "w2Ds", "M20D", "OD", "L", "Q", "w3Dp", "w2Cd",
    "M21C", "w3Cs", "M30C", "w3Bd", "M31AB", "w2Dd", "M21D", "S01", "w3Ds", "M30D", "S22", "P",
    "w3Cd", "M31C", "w3Dd", "M31D", "S33",
)


def relay_kernel(
    x_hbm, q_hbm, g_hbm, pre_hbm, bound_ref, rq_hbm, rf_hbm, cq_hbm, cf_hbm,
    s_ref, pre_ref, k_ref,
    xs, gs, go, xt, acc, oacc, grad, ograd, sacc, norms, roots, col_roots, raw,
    own_sem, send_sem, x_sem, g_sem, o_sem, swap_sem,
):
    shards, parts, block, span = xs.shape
    width = go.shape[2]
    features = xt.shape[1]
    chunk = s_ref.shape[1]
    heads = width // HEAD
    f32 = jnp.float32
    fs = lax.axis_index("fs")
    tp = lax.axis_index("tp")
    z, px = lax.div(fs, 2), lax.rem(fs, 2)
    py, pc = lax.div(tp, 2), lax.rem(tp, 2)
    pair = z + 1 - 2 * lax.rem(z, 2)
    low = z < 2
    near = jnp.where(low, 2, 1)
    layer = {"A": z, "B": pair, "C": near, "D": jnp.where(low, 3, 0)}
    middle = jnp.logical_and(z > 0, z < 3)
    flips = {"c": (0, 0), "p": (1 - pc, pc), "s": (pc, 1 - pc), "d": (1, 1)}

    def column(who):
        flip_x, flip_y = flips[who]
        return px + flip_x - 2 * px * flip_x, py + flip_y - 2 * py * flip_y

    def device(link):
        if link in ("b", "n"):
            return (2 * pair + px, tp)
        if link == "m":
            return (2 * near + px, tp)
        if link == "core":
            return (fs, tp + 1 - 2 * pc)
        x, y = column(link)
        return (2 * z + x, 2 * y + pc)

    beside = {link: device(link) for link in ("b", "n", "m", "p", "s", "core")}
    conds = {"n": middle, "m": middle}

    def guarded(cond, action):
        if cond is None:
            action()
        else:
            pl.when(cond)(action)

    barrier = pltpu.get_barrier_semaphore()

    def greet(name):
        pl.semaphore_signal(barrier, inc=1, device_id=beside[name], device_id_type=MESH)

    for name in ("b", "p", "s", "core"):
        greet(name)
    guarded(middle, lambda: greet("m"))
    loads = [
        pltpu.make_async_copy(source, target, own_sem.at[number])
        for number, (source, target) in enumerate(
            (
                (x_hbm, xs.at[fs, tp]),
                (q_hbm, raw.at[0]),
                (g_hbm, raw.at[1]),
                (pre_hbm, raw.at[2]),
                (rq_hbm, roots.at[0]),
                (rf_hbm, roots.at[1]),
                (cq_hbm, col_roots.at[0]),
                (cf_hbm, col_roots.at[1]),
            )
        )
    ]
    for load in loads:
        load.start()
    for load in loads[1:4]:
        load.wait()
    sigma_gate = jax.nn.sigmoid(raw[2].astype(f32))
    cot = to_bf16(
        raw[1].astype(f32) * (1.0 - bound_ref[...]) * sigma_gate * (1.0 - sigma_gate)
    )

    @pl.when(pc == 0)
    def _():
        gs[fs, py, 0] = raw[0]
        go[fs] = cot

    @pl.when(pc == 1)
    def _():
        gs[fs, py, 1] = cot
        go[fs] = raw[0]

    loads[0].wait()
    pl.semaphore_wait(barrier, 4 + jnp.where(middle, 1, 0))

    half_rows = block // 2
    pending = []
    dones = []

    def halves(phase):
        return 1 - pc if phase == 2 else pc

    def piece(phase, name):
        x, y = column(name[1])
        shard = 2 * layer[name[0]] + x
        if phase < 2:
            rows = pl.ds(phase * half_rows, half_rows)
            part = 2 * y + pc
            return xs.at[shard, part, rows], x_sem.at[phase, shard, part]
        return gs.at[shard, y, halves(phase)], g_sem.at[phase - 2, shard, y]

    def start(src, dst, sem, link, cond=None):
        number = len(pending)

        def build():
            return pltpu.make_async_remote_copy(
                src_ref=src, dst_ref=dst, send_sem=send_sem.at[number], recv_sem=sem,
                device_id=beside[link], device_id_type=MESH,
            )

        guarded(cond, lambda: build().start())
        pending.append((cond, build))

    def landed(ref, sem):
        pltpu.make_async_remote_copy(
            src_ref=ref, dst_ref=ref, send_sem=send_sem.at[0], recv_sem=sem,
            device_id=beside["core"], device_id_type=MESH,
        ).wait_recv()

    def forward(phase, name):
        here, sem = piece(phase, name)
        for link in ROUTES.get(name, ()):
            start(here, here, sem, link, conds.get(link))
        if phase < 2:
            start(here, here, sem, "core")
        if phase == 2 and name != "Ac" and name[1] != "d":
            cond = {"c": None, "p": pc == 0, "s": pc == 1}[name[1]]
            shard = 2 * layer[name[0]] + column(name[1])[0]
            start(here, go.at[shard], o_sem.at[shard], "core", cond)

    start(go.at[fs], gs.at[fs, py, pc], g_sem.at[0, fs, py], "core")

    def from_core(label):
        for phase in range(2):
            for x in range(2):
                for y in range(2):
                    shard, part = 2 * layer[label] + x, 2 * y + 1 - pc
                    rows = pl.ds(phase * half_rows, half_rows)
                    landed(xs.at[shard, part, rows], x_sem.at[phase, shard, part])

    def transpose(label):
        at = LAYERS.index(label)
        for x in range(2):
            for part in range(parts):
                turned = xs[2 * layer[label] + x, part].T
                xt[at, part * span : (part + 1) * span, x * block : (x + 1) * block] = turned

    squares = []
    tile = 512
    steps = features // tile

    def multiply(labels, block_of, into, out, lanes, first, final):
        def body(step, total):
            rows = pl.ds(pl.multiple_of(step * tile, tile), tile)
            value = None
            for label in labels:
                product = wide_dot(xt[LAYERS.index(label), rows, :], block_of(label), ((1,), (0,)))
                value = product if value is None else value + product
            if not first:
                value = value + into[rows, :]
            if final:
                out[rows, lanes] = to_bf16(value)
                squared = (value * value).reshape(tile // 8, 8, width)
                return total + jnp.sum(squared, axis=0)
            into[rows, :] = value
            return total

        total = lax.fori_loop(0, steps, body, jnp.zeros((8, width), f32))
        if final:
            squares.append(total)

    def own_block(phase, far):
        y = 1 - py if far else py

        def block_of(label):
            both = pl.ds(2 * layer[label], 2)
            return gs[both, y, halves(phase)].reshape(2 * block, width)

        return block_of

    def other_block(label):
        return go[pl.ds(2 * layer[label], 2)].reshape(2 * block, width)

    mine = pl.ds(pl.multiple_of(fs * chunk, chunk), chunk)
    size = float(features * grad.shape[1])

    def outer_step(lanes, first, final):
        wide = 2 * chunk
        if final:
            square = jnp.sum(squares[0], axis=(0, 1), keepdims=True)
            for more in squares[1:]:
                square = square + jnp.sum(more, axis=(0, 1), keepdims=True)
            norms[0] = jnp.broadcast_to(square, norms.shape[1:])
            scale = (1.0 - stat_decay) / grad.shape[1] * (size / (square + 1.0))
            swap_norm = pltpu.make_async_remote_copy(
                src_ref=norms.at[0], dst_ref=norms.at[1],
                send_sem=swap_sem.at[0], recv_sem=swap_sem.at[1],
                device_id=beside["core"], device_id_type=MESH,
            )
        left = grad[mine, lanes]
        for step in range(features // wide):
            rows = slice(step * wide, (step + 1) * wide)
            product = wide_dot(left, grad[rows, lanes], ((1,), (1,)))
            if not first:
                product = product + sacc[:, rows]
            if not final:
                sacc[:, rows] = product
                continue
            s_ref[pc, :, rows] = to_bf16(product * scale)
            if step == 0:
                swap_norm.start()
                dones.append(swap_norm)
            else:
                send_outer(step - 1)
        if final:
            send_outer(features // wide - 1)

    def outer_copy(which, step):
        rows = pl.ds(step * 2 * chunk, 2 * chunk)
        return pltpu.make_async_remote_copy(
            src_ref=s_ref.at[which, :, rows], dst_ref=s_ref.at[which, :, rows],
            send_sem=swap_sem.at[2 + step], recv_sem=swap_sem.at[6 + step],
            device_id=beside["core"], device_id_type=MESH,
        )

    def send_outer(step):
        outer_copy(pc, step).start()
        dones.append(step)

    def products(which, source, lanes):
        left = wide_dot(roots[which], source[:, lanes], ((1,), (0,)))

        def body(step, sums):
            rows = pl.ds(pl.multiple_of(step * chunk, chunk), chunk)
            outs = []
            for head in range(heads):
                start_lane = lanes.start + head * HEAD
                part = source[rows, start_lane : start_lane + HEAD]
                outs.append(sums[head] + wide_dot(part, part, ((0,), (0,))))
            return tuple(outs)

        sums = lax.fori_loop(
            0, features // chunk, body, tuple(jnp.zeros((HEAD, HEAD), f32) for _ in range(heads))
        )
        for head in range(heads):
            at = slice(head * HEAD, (head + 1) * HEAD)
            k_ref[which, head] = sums[head]
            pre_ref[which, :, at] = wide_dot(
                to_bf16(left[:, at]), col_roots[which, head], ((1,), (0,))
            )

    everything = slice(0, width)
    for op in PROGRAM:
        kind, rest = op[0], op[1:]
        if kind == "o":
            phase = int(rest)
            if phase == 2:
                landed(*piece(phase, "Ac"))
            forward(phase, "Ac")
        elif kind == "w":
            phase, name = int(rest[0]), rest[1:]
            landed(*piece(phase, name))
            forward(phase, name)
        elif kind == "T":
            from_core(rest)
            transpose(rest)
        elif kind == "M":
            phase, far, labels = int(rest[0]), int(rest[1]), rest[2:]
            at = 2 * (phase - 2) + far
            lanes = slice(at * width, (at + 1) * width)
            multiply(
                labels, own_block(phase, far), acc.at[at], grad, lanes,
                labels[0] == "A", labels[-1] == "D",
            )
        elif kind == "O":
            for label in rest:
                for x in range(2):
                    shard = 2 * layer[label] + x
                    if label == "A":
                        @pl.when(px != x)
                        def _():
                            landed(go.at[shard], o_sem.at[shard])
                    else:
                        landed(go.at[shard], o_sem.at[shard])
            multiply(
                rest, other_block, oacc, ograd, everything, rest[0] == "A", rest[-1] == "D"
            )
            if rest[-1] == "D":
                squares.pop()
        elif kind == "S":
            first, last = int(rest[0]), int(rest[1])
            outer_step(slice(first * width, (last + 1) * width), first == 0, last == 3)
        elif kind == "L":
            for load in loads[4:]:
                load.wait()
        elif kind == "P":
            products(pc, grad, slice(2 * width, 3 * width))
        elif kind == "Q":
            products(1 - pc, ograd, everything)

    dones[0].wait()
    mine_sum, their_sum = norms[0, 0:1, 0:1], norms[1, 0:1, 0:1]
    sums = (
        jnp.where(pc == 0, mine_sum, their_sum),
        jnp.where(pc == 0, their_sum, mine_sum),
    )
    for which in range(2):
        scale_twice = size / (sums[which] + 1.0)
        pre_ref[which] = pre_ref[which] * jnp.sqrt(scale_twice)
        for head in range(heads):
            k_ref[which, head] = k_ref[which, head] * (
                (1.0 - stat_decay) / features * scale_twice
            )
    for step in dones[1:]:
        outer_copy(pc, step).wait_send()
        outer_copy(1 - pc, step).wait_recv()
    for cond, build in pending:
        guarded(cond, lambda build=build: build().wait_send())


def relayed_products(
    x, query_grad, forget_grad, forget_pre, lower_bound,
    query_root, forget_root, query_col_root, forget_col_root,
):
    shards, parts = lax.axis_size("fs"), lax.axis_size("tp")
    block, span = x.shape
    width = query_grad.shape[1]
    chunk, features = query_root.shape
    bf16, f32 = jnp.bfloat16, jnp.float32
    heads = query_col_root.shape
    vmem = pl.BlockSpec(memory_space=pltpu.VMEM)
    hbm = pl.BlockSpec(memory_space=pltpu.HBM)
    return pl.pallas_call(
        relay_kernel,
        out_shape=[
            jax.ShapeDtypeStruct((2, chunk, features), bf16),
            jax.ShapeDtypeStruct((2, chunk, width), f32),
            jax.ShapeDtypeStruct((2,) + heads, f32),
        ],
        in_specs=[hbm] * 4 + [vmem] + [hbm] * 4,
        out_specs=[vmem] * 3,
        scratch_shapes=[
            pltpu.VMEM((shards, parts, block, span), bf16),
            pltpu.VMEM((shards, 2, 2, block, width), bf16),
            pltpu.VMEM((shards, block, width), bf16),
            pltpu.VMEM((shards // 2, features, 2 * block), bf16),
            pltpu.VMEM((4, features, width), f32),
            pltpu.VMEM((features, width), f32),
            pltpu.VMEM((features, parts * width), bf16),
            pltpu.VMEM((features, width), bf16),
            pltpu.VMEM((chunk, features), f32),
            pltpu.VMEM((2, 8, 128), f32),
            pltpu.VMEM((2, chunk, features), bf16),
            pltpu.VMEM((2,) + heads, bf16),
            pltpu.VMEM((3, block, width), bf16),
            pltpu.SemaphoreType.DMA((8,)),
            pltpu.SemaphoreType.DMA((128,)),
            pltpu.SemaphoreType.DMA((2, shards, parts)),
            pltpu.SemaphoreType.DMA((2, shards, 2)),
            pltpu.SemaphoreType.DMA((shards,)),
            pltpu.SemaphoreType.DMA((10,)),
        ],
        compiler_params=pltpu.CompilerParams(
            collective_id=0, has_side_effects=True, vmem_limit_bytes=61 * 1024 * 1024
        ),
    )(
        x, query_grad, forget_grad, forget_pre, lower_bound.reshape(1, -1),
        query_root, forget_root, query_col_root, forget_col_root,
    )


def finish_kernel(outer_ref, pre_ref, column_ref, *refs):
    weights, moments, rows, cols = (refs[2 * k : 2 * k + 2] for k in range(4))
    outs = refs[8:]
    for which in range(2):
        master_ref, copy_ref, step_ref, moment_ref, rows_ref, cols_ref = outs[which::2]
        precond = pre_ref[which]
        moment_next = moment_decay * moments[which][...] + (1.0 - moment_decay) * precond
        update_step = moment_decay * moment_next + (1.0 - moment_decay) * precond
        master = weights[which][...] - learn_rate * update_step
        master_ref[...] = master
        copy_ref[...] = to_bf16(master)
        step_ref[...] = update_step
        moment_ref[...] = moment_next
        rows_ref[...] = stat_decay * rows[which][...] + outer_ref[which].astype(jnp.float32)
        cols_ref[...] = stat_decay * cols[which][...] + column_ref[which]


def finished(outers, pres, columns, weights, moments, rows, cols):
    f32, bf16 = jnp.float32, jnp.bfloat16
    chunk, width = weights[0].shape
    features = rows[0].shape[1]
    heads = cols[0].shape
    steps = 2
    tile = chunk // steps
    narrow = pl.BlockSpec((tile, width), lambda i: (i, 0))
    wide = pl.BlockSpec((tile, features), lambda i: (i, 0))
    head = pl.BlockSpec((heads[0], heads[1] // steps, heads[2]), lambda i: (0, i, 0))
    both = pl.BlockSpec((2, tile, features), lambda i: (0, i, 0))
    both_narrow = pl.BlockSpec((2, tile, width), lambda i: (0, i, 0))
    both_head = pl.BlockSpec(
        (2, heads[0], heads[1] // steps, heads[2]), lambda i: (0, 0, i, 0)
    )
    flat = lambda kind: [jax.ShapeDtypeStruct((chunk, width), kind)] * 2
    return pl.pallas_call(
        finish_kernel,
        grid=(steps,),
        out_shape=flat(f32)
        + flat(bf16)
        + flat(f32)
        + flat(f32)
        + [jax.ShapeDtypeStruct((chunk, features), f32)] * 2
        + [jax.ShapeDtypeStruct(heads, f32)] * 2,
        in_specs=[both, both_narrow, both_head] + [narrow] * 4 + [wide] * 2 + [head] * 2,
        out_specs=[narrow] * 8 + [wide] * 2 + [head] * 2,
        compiler_params=pltpu.CompilerParams(vmem_limit_bytes=61 * 1024 * 1024),
    )(outers, pres, columns, *weights, *moments, *rows, *cols)


def gather_plan(
    inputs,
    query_grad,
    forget_grad,
    forget_pre,
    lower_bound,
    query_weight,
    forget_weight,
    query_moment,
    forget_moment,
    query_rows,
    forget_rows,
    query_cols,
    forget_cols,
    query_row_root,
    forget_row_root,
    query_col_root,
    forget_col_root,
):
    outers, pres, columns = relayed_products(
        inputs,
        query_grad,
        forget_grad,
        forget_pre,
        lower_bound,
        query_row_root,
        forget_row_root,
        query_col_root,
        forget_col_root,
    )
    return tuple(
        finished(
            outers,
            pres,
            columns,
            (query_weight, forget_weight),
            (query_moment, forget_moment),
            (query_rows, forget_rows),
            (query_cols, forget_cols),
        )
    )


def on_device(*args):
    token_count = args[0].shape[0] * lax.axis_size("fs")
    feature_count = args[0].shape[1] * lax.axis_size("tp")
    paired = lax.axis_size("fs") == 8 and lax.axis_size("tp") == 4
    if paired and token_count <= feature_count:
        return gather_plan(*args)
    return reduce_plan(*args)


def solution(mesh):
    in_specs = (
        P("fs", "tp"),
        P("fs", "tp"),
        P("fs", "tp"),
        P("fs", "tp"),
        P("tp"),
        P("fs", "tp"),
        P("fs", "tp"),
        P("fs", "tp"),
        P("fs", "tp"),
        P("fs", None),
        P("fs", None),
        P("tp", None, None),
        P("tp", None, None),
        P("fs", None),
        P("fs", None),
        P("tp", None, None),
        P("tp", None, None),
    )
    out_specs = (
        P("fs", "tp"),
        P("fs", "tp"),
        P("fs", "tp"),
        P("fs", "tp"),
        P("fs", "tp"),
        P("fs", "tp"),
        P("fs", "tp"),
        P("fs", "tp"),
        P("fs", None),
        P("fs", None),
        P("tp", None, None),
        P("tp", None, None),
    )
    return jax.shard_map(
        on_device, mesh=mesh, in_specs=in_specs, out_specs=out_specs, check_vma=False
    )
```

time: 66.3 us -> 70.9 us (1.069)
  Pallas kernels: 65.3 us -> 70.1 us
    pallas_call x1, Pallas kernels: 58.1 us -> 64.6 us  [relayed_products(): pl.pallas_call(relay_kernel, out_shape=[jax.ShapeDtypeStruct((2, chunk, f...]
    pallas_call x1 -> x0, Pallas kernels: 1.61 us -> none  [packed_cotangents(): pl.pallas_call(pack_kernel, out_shape=jax.ShapeDtypeStruct((2,) + query_g...]
where the time goes in v1:
time: 70.9 us; the launch traced here: 70.8 us
  Pallas kernels  70.1 us (99%)
    pallas_call x1, Pallas kernels, relayed_products(): pl.pallas_call(relay_kernel, out_shape=[jax.ShapeDtypeStruct((2, chunk, f...  64.6 us
    pallas_call x1, Pallas kernels, finished(): pl.pallas_call(finish_kernel, grid=(steps,), out_shape=flat(f32) + flat(b...  5.52 us

profile of v1, /device:TPU:0, one launch (start us, length us, event | category | flops | bytes accessed | tf_op | source)
XLA Modules:
  0.0 70.8 jit_solution(2765388933283955494)
XLA Ops:
  0.6 64.6 %shard_map.256 = (bf16[2,256,2048]{2,1,0:T(8,128)(2,1)}, f32[2,256,256]{2,1,0:T(8,128)}, f32[2,2,128,128]{3,2,1,0:T(8,128)}) custom-call(bf16[128,512]{1,0:T(8,128)(2,1)} %x_hbm.1, bf16[128,256]{1,0:T(8,128)(2,1)} %q_hbm.1, bf16[128,256]{1,0:T(8,128)(2,1)} %g_hbm.1, bf16[128,256]{1,0:T(8,128)(2,1)} %pre_hbm.1, f32[1,256]{1,0:T(1,128)} %bitcast.1, ...), custom_call_target="tpu_custom_call" | custom-call | tf_op jit(solution)/shard_map/pallas_call | solution.py:530
  65.2 5.5 %shard_map.257 = (f32[256,256]{1,0:T(8,128)}, f32[256,256]{1,0:T(8,128)}, bf16[256,256]{1,0:T(8,128)(2,1)}, bf16[256,256]{1,0:T(8,128)(2,1)}, f32[256,256]{1,0:T...) custom-call(bf16[2,256,2048]{2,1,0:T(8,128)(2,1)} %get-tuple-element, ...), custom_call_target="tpu_custom_call" | custom-call | tf_op jit(solution)/shard_map/pallas_call | solution.py:602

commit v2 on v1

--- a/solution.py
+++ b/solution.py
@@ -1,5 +1,3 @@
-import functools
-
 import jax
 import jax.numpy as jnp
 from jax import lax
@@ -166,7 +164,6 @@
 
 
 LAYERS = "ABCD"
-ACROSS = {"p": {"c": "p", "p": "c", "s": "d", "d": "s"}, "s": {"c": "s", "s": "c", "p": "d", "d": "p"}}
 ROUTES = {
     "Ac": ("b", "m", "p", "s"),
     "Bc": ("m", "s"),
@@ -178,26 +175,26 @@
     "Ad": ("b",),
 }
 PROGRAM = (
-    "o0", "o1", "w0Ap", "w0As", "w0Bc", "w1Ap", "w1As", "w1Bc", "w0Cc", "w0Bp", "w0Ad", "w0Bs",
-    "w1Cc", "w0Cp", "w0Cs", "w1Bp", "w0Dc", "w1Ad", "TA", "w1Bs", "o2", "w1Cp", "w1Dc", "w0Bd",
-    "w0Dp", "o3", "w2Ap", "w1Cs", "w0Cd", "w1Bd", "TB", "w1Dp", "w2Bc", "w0Ds", "w2Cc", "w2As",
-    "w3Ap", "w1Cd", "TC", "w1Ds", "w2Bp", "w3Bc", "w2Cp", "w2Dc", "w0Dd", "w2Ad", "w3Cc", "w3As",
-    "w1Dd", "TD", "w2Bs", "M20AB", "OAB", "w2Dp", "w3Bp", "w3Dc", "w2Cs", "M20C", "OC", "w3Cp",
-    "w3Ad", "w2Bd", "M21AB", "w3Bs", "M30AB", "w2Ds", "M20D", "OD", "L", "Q", "w3Dp", "w2Cd",
-    "M21C", "w3Cs", "M30C", "w3Bd", "M31AB", "w2Dd", "M21D", "S01", "w3Ds", "M30D", "S22", "P",
-    "w3Cd", "M31C", "w3Dd", "M31D", "S33",
+    "o0", "o2", "o1", "o3", "w2Cc", "w0Bc", "w2Ap", "w1Cc", "w3Bc", "w2Bc", "w1Ap", "w0Cc",
+    "w2Cp", "w1Bc", "w1Cp", "w0Ap", "w3Dc", "w0Cp", "w2Bs", "w3As", "w3Ap", "w1Ad", "w0Dc",
+    "w0Bp", "w1Cs", "w1Dc", "w3Bs", "w0As", "w3Bp", "w0Cs", "w1Bs", "w3Dp", "w0Ad", "w2Cd",
+    "w2As", "w1As", "TA", "w1Bp", "w2Cs", "w3Cc", "w0Bs", "w0Cd", "w2Dc", "w0Bd", "w2Ad", "w1Dp",
+    "w1Cd", "TC", "w3Ad", "w0Ds", "w0Dp", "w3Cp", "w1Bd", "TB", "w3Ds", "w2Bp", "w2Bd",
+    ("G2ABC", ("w2Dp",), ("w3Dd",), ("w0Dd",)), "w2Ds", "w1Dd", "w3Bd", "w3Cs", "w3Cd",
+    ("G3ABC", ("w1Ds",), ("w2Dd",)), "TD", ("G2D",), "S01", "L", "Q", ("G3D",), "S23", "P",
 )
 
 
 def relay_kernel(
     x_hbm, q_hbm, g_hbm, pre_hbm, bound_ref, rq_hbm, rf_hbm, cq_hbm, cf_hbm,
-    s_ref, pre_ref, k_ref,
-    xs, gs, go, xt, acc, oacc, grad, ograd, sacc, norms, roots, col_roots, raw,
+    wq_hbm, wf_hbm, mq_hbm, mf_hbm, hq_hbm, hf_hbm, vq_hbm, vf_hbm,
+    s_ref, pre_ref, k_ref, weight_ref, moment_ref, rows_ref, cols_ref,
+    xs, gs, go, xt, acc, grad, sacc, norms, roots, col_roots, raw, turn,
     own_sem, send_sem, x_sem, g_sem, o_sem, swap_sem,
 ):
     shards, parts, block, span = xs.shape
     width = go.shape[2]
-    features = xt.shape[1]
+    features = xt.shape[0]
     chunk = s_ref.shape[1]
     heads = width // HEAD
     f32 = jnp.float32
@@ -228,6 +225,7 @@
 
     beside = {link: device(link) for link in ("b", "n", "m", "p", "s", "core")}
     conds = {"n": middle, "m": middle}
+    aside = {"c": None, "p": pc == 0, "s": pc == 1}
 
     def guarded(cond, action):
         if cond is None:
@@ -255,10 +253,18 @@
                 (rf_hbm, roots.at[1]),
                 (cq_hbm, col_roots.at[0]),
                 (cf_hbm, col_roots.at[1]),
+                (wq_hbm, weight_ref.at[0]),
+                (wf_hbm, weight_ref.at[1]),
+                (mq_hbm, moment_ref.at[0]),
+                (mf_hbm, moment_ref.at[1]),
+                (hq_hbm, rows_ref.at[0]),
+                (hf_hbm, rows_ref.at[1]),
+                (vq_hbm, cols_ref.at[0]),
+                (vf_hbm, cols_ref.at[1]),
             )
         )
     ]
-    for load in loads:
+    for load in loads[:4]:
         load.start()
     for load in loads[1:4]:
         load.wait()
@@ -280,6 +286,8 @@
     loads[0].wait()
     pl.semaphore_wait(barrier, 4 + jnp.where(middle, 1, 0))
 
+    for load in loads[4:]:
+        load.start()
     half_rows = block // 2
     pending = []
     dones = []
@@ -296,10 +304,11 @@
             return xs.at[shard, part, rows], x_sem.at[phase, shard, part]
         return gs.at[shard, y, halves(phase)], g_sem.at[phase - 2, shard, y]
 
-    def start(src, dst, sem, link, cond=None):
+    def start(recipe, link, cond=None):
         number = len(pending)
 
         def build():
+            src, dst, sem = recipe()
             return pltpu.make_async_remote_copy(
                 src_ref=src, dst_ref=dst, send_sem=send_sem.at[number], recv_sem=sem,
                 device_id=beside[link], device_id_type=MESH,
@@ -315,17 +324,23 @@
         ).wait_recv()
 
     def forward(phase, name):
-        here, sem = piece(phase, name)
+        def same():
+            here, sem = piece(phase, name)
+            return here, here, sem
+
+        def beyond():
+            here, _ = piece(phase, name)
+            shard = 2 * layer[name[0]] + column(name[1])[0]
+            return here, go.at[shard], o_sem.at[shard]
+
         for link in ROUTES.get(name, ()):
-            start(here, here, sem, link, conds.get(link))
+            start(same, link, conds.get(link))
         if phase < 2:
-            start(here, here, sem, "core")
+            start(same, "core")
         if phase == 2 and name != "Ac" and name[1] != "d":
-            cond = {"c": None, "p": pc == 0, "s": pc == 1}[name[1]]
-            shard = 2 * layer[name[0]] + column(name[1])[0]
-            start(here, go.at[shard], o_sem.at[shard], "core", cond)
-
-    start(go.at[fs], gs.at[fs, py, pc], g_sem.at[0, fs, py], "core")
+            start(beyond, "core", aside[name[1]])
+
+    start(lambda: (go.at[fs], gs.at[fs, py, pc], g_sem.at[0, fs, py]), "core")
 
     def from_core(label):
         for phase in range(2):
@@ -337,49 +352,72 @@
 
     def transpose(label):
         at = LAYERS.index(label)
-        for x in range(2):
+
+        @pl.loop(0, 2)
+        def _(x):
+            lanes = pl.ds(pl.multiple_of((2 * at + x) * block, block), block)
             for part in range(parts):
                 turned = xs[2 * layer[label] + x, part].T
-                xt[at, part * span : (part + 1) * span, x * block : (x + 1) * block] = turned
+                xt[part * span : (part + 1) * span, lanes] = turned
 
     squares = []
-    tile = 512
-    steps = features // tile
-
-    def multiply(labels, block_of, into, out, lanes, first, final):
+    tile = features // 4
+
+    def own_block(phase, far, label):
+        y = 1 - py if far else py
+        both = pl.ds(2 * layer[label], 2)
+        return gs[both, y, halves(phase)].reshape(2 * block, width)
+
+    def other_block(label):
+        return go[pl.ds(2 * layer[label], 2)].reshape(2 * block, width)
+
+    def gradients(phase, labels, events):
+        first, final = labels[0] == LAYERS[0], labels[-1] == LAYERS[-1]
+        start_token = LAYERS.index(labels[0]) * 2 * block
+        tokens = slice(start_token, start_token + len(labels) * 2 * block)
+        if phase == 2:
+            for label in labels:
+                for x in range(2):
+                    shard = 2 * layer[label] + x
+                    guarded(
+                        px != x if label == "A" else None,
+                        lambda shard=shard: landed(go.at[shard], o_sem.at[shard]),
+                    )
+
         def body(step, total):
             rows = pl.ds(pl.multiple_of(step * tile, tile), tile)
-            value = None
-            for label in labels:
-                product = wide_dot(xt[LAYERS.index(label), rows, :], block_of(label), ((1,), (0,)))
-                value = product if value is None else value + product
-            if not first:
-                value = value + into[rows, :]
-            if final:
-                out[rows, lanes] = to_bf16(value)
-                squared = (value * value).reshape(tile // 8, 8, width)
-                return total + jnp.sum(squared, axis=0)
-            into[rows, :] = value
+            for far in range(3 if phase == 2 else 2):
+                at = 4 if far == 2 else 2 * (phase - 2) + far
+                right = jnp.concatenate(
+                    [other_block(k) if far == 2 else own_block(phase, far, k) for k in labels], axis=0
+                )
+                value = wide_dot(xt[rows, tokens], right, ((1,), (0,)))
+                if not first:
+                    value = value + acc[at, rows, :]
+                if final:
+                    grad[rows, at * width : (at + 1) * width] = to_bf16(value)
+                    if far < 2:
+                        squared = (value * value).reshape(tile // 8, 8, width)
+                        total = total + jnp.sum(squared, axis=0)
+                else:
+                    acc[at, rows, :] = value
+            for number, names in enumerate(events):
+                if names:
+
+                    @pl.when(step == number)
+                    def _(names=names):
+                        for name in names:
+                            travel(name)
+
             return total
 
-        total = lax.fori_loop(0, steps, body, jnp.zeros((8, width), f32))
+        total = lax.fori_loop(0, features // tile, body, jnp.zeros((8, width), f32))
         if final:
             squares.append(total)
 
-    def own_block(phase, far):
-        y = 1 - py if far else py
-
-        def block_of(label):
-            both = pl.ds(2 * layer[label], 2)
-            return gs[both, y, halves(phase)].reshape(2 * block, width)
-
-        return block_of
-
-    def other_block(label):
-        return go[pl.ds(2 * layer[label], 2)].reshape(2 * block, width)
-
     mine = pl.ds(pl.multiple_of(fs * chunk, chunk), chunk)
-    size = float(features * grad.shape[1])
+    hidden = parts * width
+    size = float(features * hidden)
 
     def outer_step(lanes, first, final):
         wide = 2 * chunk
@@ -388,29 +426,33 @@
             for more in squares[1:]:
                 square = square + jnp.sum(more, axis=(0, 1), keepdims=True)
             norms[0] = jnp.broadcast_to(square, norms.shape[1:])
-            scale = (1.0 - stat_decay) / grad.shape[1] * (size / (square + 1.0))
+            scale = (1.0 - stat_decay) / hidden * (size / (square + 1.0))
             swap_norm = pltpu.make_async_remote_copy(
                 src_ref=norms.at[0], dst_ref=norms.at[1],
                 send_sem=swap_sem.at[0], recv_sem=swap_sem.at[1],
                 device_id=beside["core"], device_id_type=MESH,
             )
-        left = grad[mine, lanes]
+        if not final:
+
+            @pl.loop(0, features // wide)
+            def _(step):
+                rows = pl.ds(pl.multiple_of(step * wide, wide), wide)
+                product = wide_dot(grad[mine, lanes], grad[rows, lanes], ((1,), (1,)))
+                if not first:
+                    product = product + sacc[:, rows]
+                sacc[:, rows] = product
+
+            return
         for step in range(features // wide):
             rows = slice(step * wide, (step + 1) * wide)
-            product = wide_dot(left, grad[rows, lanes], ((1,), (1,)))
-            if not first:
-                product = product + sacc[:, rows]
-            if not final:
-                sacc[:, rows] = product
-                continue
-            s_ref[pc, :, rows] = to_bf16(product * scale)
+            product = wide_dot(grad[mine, lanes], grad[rows, lanes], ((1,), (1,)))
+            s_ref[pc, :, rows] = to_bf16((product + sacc[:, rows]) * scale)
             if step == 0:
                 swap_norm.start()
                 dones.append(swap_norm)
             else:
                 send_outer(step - 1)
-        if final:
-            send_outer(features // wide - 1)
+        send_outer(features // wide - 1)
 
     def outer_copy(which, step):
         rows = pl.ds(step * 2 * chunk, 2 * chunk)
@@ -424,76 +466,44 @@
         outer_copy(pc, step).start()
         dones.append(step)
 
-    def products(which, source, lanes):
-        left = wide_dot(roots[which], source[:, lanes], ((1,), (0,)))
-
-        def body(step, sums):
-            rows = pl.ds(pl.multiple_of(step * chunk, chunk), chunk)
-            outs = []
-            for head in range(heads):
-                start_lane = lanes.start + head * HEAD
-                part = source[rows, start_lane : start_lane + HEAD]
-                outs.append(sums[head] + wide_dot(part, part, ((0,), (0,))))
-            return tuple(outs)
-
-        sums = lax.fori_loop(
-            0, features // chunk, body, tuple(jnp.zeros((HEAD, HEAD), f32) for _ in range(heads))
-        )
+    def products(which, lanes):
+        for step in range(features // chunk):
+            rows = slice(step * chunk, (step + 1) * chunk)
+            turn[:, rows] = grad[rows, lanes].T
+        left = wide_dot(roots[which], grad[:, lanes], ((1,), (0,)))
+        gram = wide_dot(turn[...], grad[:, lanes], ((1,), (0,)))
         for head in range(heads):
             at = slice(head * HEAD, (head + 1) * HEAD)
-            k_ref[which, head] = sums[head]
+            k_ref[which, head] = gram[at, at]
             pre_ref[which, :, at] = wide_dot(
                 to_bf16(left[:, at]), col_roots[which, head], ((1,), (0,))
             )
 
-    everything = slice(0, width)
+    def travel(op):
+        phase = int(op[1])
+        if op[0] == "w" or phase == 2:
+            landed(*piece(phase, op[2:] or "Ac"))
+        forward(phase, op[2:] or "Ac")
+
     for op in PROGRAM:
         kind, rest = op[0], op[1:]
-        if kind == "o":
-            phase = int(rest)
-            if phase == 2:
-                landed(*piece(phase, "Ac"))
-            forward(phase, "Ac")
-        elif kind == "w":
-            phase, name = int(rest[0]), rest[1:]
-            landed(*piece(phase, name))
-            forward(phase, name)
+        if isinstance(op, tuple):
+            gradients(int(op[0][1]), op[0][2:], op[1:])
+        elif kind in "ow":
+            travel(op)
         elif kind == "T":
             from_core(rest)
             transpose(rest)
-        elif kind == "M":
-            phase, far, labels = int(rest[0]), int(rest[1]), rest[2:]
-            at = 2 * (phase - 2) + far
-            lanes = slice(at * width, (at + 1) * width)
-            multiply(
-                labels, own_block(phase, far), acc.at[at], grad, lanes,
-                labels[0] == "A", labels[-1] == "D",
-            )
-        elif kind == "O":
-            for label in rest:
-                for x in range(2):
-                    shard = 2 * layer[label] + x
-                    if label == "A":
-                        @pl.when(px != x)
-                        def _():
-                            landed(go.at[shard], o_sem.at[shard])
-                    else:
-                        landed(go.at[shard], o_sem.at[shard])
-            multiply(
-                rest, other_block, oacc, ograd, everything, rest[0] == "A", rest[-1] == "D"
-            )
-            if rest[-1] == "D":
-                squares.pop()
         elif kind == "S":
             first, last = int(rest[0]), int(rest[1])
             outer_step(slice(first * width, (last + 1) * width), first == 0, last == 3)
         elif kind == "L":
-            for load in loads[4:]:
+            for load in loads[4:8]:
                 load.wait()
         elif kind == "P":
-            products(pc, grad, slice(2 * width, 3 * width))
+            products(pc, slice(2 * width, 3 * width))
         elif kind == "Q":
-            products(1 - pc, ograd, everything)
+            products(1 - pc, slice(4 * width, 5 * width))
 
     dones[0].wait()
     mine_sum, their_sum = norms[0, 0:1, 0:1], norms[1, 0:1, 0:1]
@@ -511,46 +521,52 @@
     for step in dones[1:]:
         outer_copy(pc, step).wait_send()
         outer_copy(1 - pc, step).wait_recv()
+    for load in loads[8:]:
+        load.wait()
     for cond, build in pending:
         guarded(cond, lambda build=build: build().wait_send())
 
 
-def relayed_products(
-    x, query_grad, forget_grad, forget_pre, lower_bound,
-    query_root, forget_root, query_col_root, forget_col_root,
-):
+def in_hbm(*arrays):
+    return [pltpu.with_memory_space_constraint(array, pltpu.HBM) for array in arrays]
+
+
+def relayed_products(x, query_grad, forget_grad, forget_pre, lower_bound, *held):
     shards, parts = lax.axis_size("fs"), lax.axis_size("tp")
     block, span = x.shape
     width = query_grad.shape[1]
-    chunk, features = query_root.shape
+    chunk, features = held[0].shape
     bf16, f32 = jnp.bfloat16, jnp.float32
-    heads = query_col_root.shape
+    heads = held[2].shape
     vmem = pl.BlockSpec(memory_space=pltpu.VMEM)
     hbm = pl.BlockSpec(memory_space=pltpu.HBM)
     return pl.pallas_call(
         relay_kernel,
         out_shape=[
-            jax.ShapeDtypeStruct((2, chunk, features), bf16),
-            jax.ShapeDtypeStruct((2, chunk, width), f32),
-            jax.ShapeDtypeStruct((2,) + heads, f32),
+            pltpu.VMEM((2, chunk, features), bf16),
+            pltpu.VMEM((2, chunk, width), f32),
+            pltpu.VMEM((2,) + heads, f32),
+            pltpu.VMEM((2, chunk, width), f32),
+            pltpu.VMEM((2, chunk, width), f32),
+            pltpu.VMEM((2, chunk, features), f32),
+            pltpu.VMEM((2,) + heads, f32),
         ],
-        in_specs=[hbm] * 4 + [vmem] + [hbm] * 4,
-        out_specs=[vmem] * 3,
+        in_specs=[hbm] * 4 + [vmem] + [hbm] * 12,
+        out_specs=[vmem] * 7,
         scratch_shapes=[
             pltpu.VMEM((shards, parts, block, span), bf16),
             pltpu.VMEM((shards, 2, 2, block, width), bf16),
             pltpu.VMEM((shards, block, width), bf16),
-            pltpu.VMEM((shards // 2, features, 2 * block), bf16),
-            pltpu.VMEM((4, features, width), f32),
-            pltpu.VMEM((features, width), f32),
-            pltpu.VMEM((features, parts * width), bf16),
-            pltpu.VMEM((features, width), bf16),
+            pltpu.VMEM((features, shards * block), bf16),
+            pltpu.VMEM((parts + 1, features, width), f32),
+            pltpu.VMEM((features, (parts + 1) * width), bf16),
             pltpu.VMEM((chunk, features), f32),
             pltpu.VMEM((2, 8, 128), f32),
             pltpu.VMEM((2, chunk, features), bf16),
             pltpu.VMEM((2,) + heads, bf16),
             pltpu.VMEM((3, block, width), bf16),
-            pltpu.SemaphoreType.DMA((8,)),
+            pltpu.VMEM((width, features), bf16),
+            pltpu.SemaphoreType.DMA((16,)),
             pltpu.SemaphoreType.DMA((128,)),
             pltpu.SemaphoreType.DMA((2, shards, parts)),
             pltpu.SemaphoreType.DMA((2, shards, 2)),
@@ -558,46 +574,46 @@
             pltpu.SemaphoreType.DMA((10,)),
         ],
         compiler_params=pltpu.CompilerParams(
-            collective_id=0, has_side_effects=True, vmem_limit_bytes=61 * 1024 * 1024
+            collective_id=0, has_side_effects=True, vmem_limit_bytes=48 * 1024 * 1024
         ),
     )(
-        x, query_grad, forget_grad, forget_pre, lower_bound.reshape(1, -1),
-        query_root, forget_root, query_col_root, forget_col_root,
-    )
-
-
-def finish_kernel(outer_ref, pre_ref, column_ref, *refs):
-    weights, moments, rows, cols = (refs[2 * k : 2 * k + 2] for k in range(4))
-    outs = refs[8:]
+        *in_hbm(x, query_grad, forget_grad, forget_pre), lower_bound.reshape(1, -1), *in_hbm(*held)
+    )
+
+
+def finish_kernel(outer_ref, pre_ref, column_ref, weight_ref, moment_ref, rows_ref, cols_ref, *outs):
+    step = pl.program_id(0)
+    tile, head_tile = outs[0].shape[0], outs[10].shape[1]
+    at = pl.ds(pl.multiple_of(step * tile, tile), tile)
+    head_at = pl.ds(pl.multiple_of(step * head_tile, head_tile), head_tile)
     for which in range(2):
-        master_ref, copy_ref, step_ref, moment_ref, rows_ref, cols_ref = outs[which::2]
-        precond = pre_ref[which]
-        moment_next = moment_decay * moments[which][...] + (1.0 - moment_decay) * precond
+        master_out, copy_out, step_out, moment_out, rows_out, cols_out = outs[which::2]
+        precond = pre_ref[which, at, :]
+        moment_next = moment_decay * moment_ref[which, at, :] + (1.0 - moment_decay) * precond
         update_step = moment_decay * moment_next + (1.0 - moment_decay) * precond
-        master = weights[which][...] - learn_rate * update_step
-        master_ref[...] = master
-        copy_ref[...] = to_bf16(master)
-        step_ref[...] = update_step
-        moment_ref[...] = moment_next
-        rows_ref[...] = stat_decay * rows[which][...] + outer_ref[which].astype(jnp.float32)
-        cols_ref[...] = stat_decay * cols[which][...] + column_ref[which]
-
-
-def finished(outers, pres, columns, weights, moments, rows, cols):
+        master = weight_ref[which, at, :] - learn_rate * update_step
+        master_out[...] = master
+        copy_out[...] = to_bf16(master)
+        step_out[...] = update_step
+        moment_out[...] = moment_next
+        rows_out[...] = stat_decay * rows_ref[which, at, :] + outer_ref[which, at, :].astype(
+            jnp.float32
+        )
+        cols_out[...] = (
+            stat_decay * cols_ref[which, :, head_at, :] + column_ref[which, :, head_at, :]
+        )
+
+
+def finished(held):
     f32, bf16 = jnp.float32, jnp.bfloat16
-    chunk, width = weights[0].shape
-    features = rows[0].shape[1]
-    heads = cols[0].shape
-    steps = 2
+    _, chunk, features = held[0].shape
+    width = held[1].shape[2]
+    heads = held[2].shape[1:]
+    steps = 4
     tile = chunk // steps
     narrow = pl.BlockSpec((tile, width), lambda i: (i, 0))
     wide = pl.BlockSpec((tile, features), lambda i: (i, 0))
     head = pl.BlockSpec((heads[0], heads[1] // steps, heads[2]), lambda i: (0, i, 0))
-    both = pl.BlockSpec((2, tile, features), lambda i: (0, i, 0))
-    both_narrow = pl.BlockSpec((2, tile, width), lambda i: (0, i, 0))
-    both_head = pl.BlockSpec(
-        (2, heads[0], heads[1] // steps, heads[2]), lambda i: (0, 0, i, 0)
-    )
     flat = lambda kind: [jax.ShapeDtypeStruct((chunk, width), kind)] * 2
     return pl.pallas_call(
         finish_kernel,
@@ -608,10 +624,10 @@
         + flat(f32)
         + [jax.ShapeDtypeStruct((chunk, features), f32)] * 2
         + [jax.ShapeDtypeStruct(heads, f32)] * 2,
-        in_specs=[both, both_narrow, both_head] + [narrow] * 4 + [wide] * 2 + [head] * 2,
+        in_specs=[pl.BlockSpec(memory_space=pltpu.VMEM)] * 7,
         out_specs=[narrow] * 8 + [wide] * 2 + [head] * 2,
-        compiler_params=pltpu.CompilerParams(vmem_limit_bytes=61 * 1024 * 1024),
-    )(outers, pres, columns, *weights, *moments, *rows, *cols)
+        compiler_params=pltpu.CompilerParams(vmem_limit_bytes=24 * 1024 * 1024),
+    )(*[pltpu.with_memory_space_constraint(array, pltpu.VMEM) for array in held])
 
 
 def gather_plan(
@@ -633,7 +649,7 @@
     query_col_root,
     forget_col_root,
 ):
-    outers, pres, columns = relayed_products(
+    held = relayed_products(
         inputs,
         query_grad,
         forget_grad,
@@ -643,18 +659,16 @@
         forget_row_root,
         query_col_root,
         forget_col_root,
-    )
-    return tuple(
-        finished(
-            outers,
-            pres,
-            columns,
-            (query_weight, forget_weight),
-            (query_moment, forget_moment),
-            (query_rows, forget_rows),
-            (query_cols, forget_cols),
-        )
-    )
+        query_weight,
+        forget_weight,
+        query_moment,
+        forget_moment,
+        query_rows,
+        forget_rows,
+        query_cols,
+        forget_cols,
+    )
+    return tuple(finished(held))
 
 
 def on_device(*args):

time: 70.9 us -> 58.2 us (0.82)
  Pallas kernels: 70.1 us -> 57.4 us
    pallas_call x1, Pallas kernels: 64.6 us -> 54.3 us  [relayed_products(): pl.pallas_call(relay_kernel, out_shape=[pltpu.VMEM((2, chunk, features),...]
    pallas_call x1, Pallas kernels: 5.52 us -> 3.03 us  [finished(): pl.pallas_call(finish_kernel, grid=(steps,), out_shape=flat(f32) + flat(b...]
where the time goes in v2:
time: 58.2 us; the launch traced here: 58 us
  Pallas kernels  57.4 us (99%)
  between operations  0.66 us (1%)
    pallas_call x1, Pallas kernels, relayed_products(): pl.pallas_call(relay_kernel, out_shape=[pltpu.VMEM((2, chunk, features),...  54.3 us
    pallas_call x1, Pallas kernels, finished(): pl.pallas_call(finish_kernel, grid=(steps,), out_shape=flat(f32) + flat(b...  3.03 us

profile of v2, /device:TPU:0, one launch (start us, length us, event | category | flops | bytes accessed | tf_op | source)
XLA Modules:
  0.0 58.0 jit_solution(14127432001751047627)
XLA Ops:
  0.7 54.3 %shard_map.256 = (bf16[2,256,2048]{2,1,0:T(8,128)(2,1)S(1)}, f32[2,256,256]{2,1,0:T(8,128)S(1)}, f32[2,2,128,128]{3,2,1,0:T(8,128)S(1)}, f32[2,256,256]{2,1,0:T(...) custom-call(bf16[128,512]{1,0:T(8,128)(2,1)} %x_hbm.1, ...), custom_call_target="tpu_custom_call" | custom-call | tf_op jit(solution)/shard_map/pallas_call | solution.py:543
  55.0 3.0 %shard_map.257 = (f32[256,256]{1,0:T(8,128)}, f32[256,256]{1,0:T(8,128)}, bf16[256,256]{1,0:T(8,128)(2,1)}, bf16[256,256]{1,0:T(8,128)(2,1)}, f32[256,256]{1,0:T...) custom-call(bf16[2,256,2048]{2,1,0:T(8,128)(2,1)S(1)} %get-tuple-ele, ...), custom_call_target="tpu_custom_call" | custom-call | tf_op jit(solution)/shard_map/pallas_call | solution.py:618

commit v3 on v2

--- a/solution.py
+++ b/solution.py
@@ -175,21 +175,21 @@
     "Ad": ("b",),
 }
 PROGRAM = (
-    "o0", "o2", "o1", "o3", "w2Cc", "w0Bc", "w2Ap", "w1Cc", "w3Bc", "w2Bc", "w1Ap", "w0Cc",
-    "w2Cp", "w1Bc", "w1Cp", "w0Ap", "w3Dc", "w0Cp", "w2Bs", "w3As", "w3Ap", "w1Ad", "w0Dc",
-    "w0Bp", "w1Cs", "w1Dc", "w3Bs", "w0As", "w3Bp", "w0Cs", "w1Bs", "w3Dp", "w0Ad", "w2Cd",
-    "w2As", "w1As", "TA", "w1Bp", "w2Cs", "w3Cc", "w0Bs", "w0Cd", "w2Dc", "w0Bd", "w2Ad", "w1Dp",
-    "w1Cd", "TC", "w3Ad", "w0Ds", "w0Dp", "w3Cp", "w1Bd", "TB", "w3Ds", "w2Bp", "w2Bd",
-    ("G2ABC", ("w2Dp",), ("w3Dd",), ("w0Dd",)), "w2Ds", "w1Dd", "w3Bd", "w3Cs", "w3Cd",
-    ("G3ABC", ("w1Ds",), ("w2Dd",)), "TD", ("G2D",), "S01", "L", "Q", ("G3D",), "S23", "P",
+    "o0", "o1", "C", "o3", "o2", "w0Bc", "w0Cc", "w1Bc", "w0Ap", "w2Bc", "w0As", "w3Cc", "w1As",
+    "w1Cc", "w1Ap", "w0Dc", "w0Cp", "w0Ad", "w2Ap", "w1Cp", "w1Bs", "w1Cs", "w3Bc", "w2Cc",
+    "w0Cs", "w1Dc", "w2Dc", "w1Cd", "w3Cs", "w2Cp", "w0Bs", "w2Bs", "w0Cd", "w3Cp", "w0Ds",
+    "w2Bp", "w1Ad", "TC", "TA", "w1Bp", "w3Dc", "w2Ad", "w1Dp", "w0Bd", "w1Ds", "w3Bs", "w0Dp",
+    "w0Bp", "w2Cs", "w1Bd", "w3As", "w2As", "TB", "w3Cd", "w3Ap", "w2Dp", "w2Cd", "w2Ds", "w2Bd",
+    ("G2ABC", ("w3Ds",), ("w1Dd",), ("w0Dd", "w3Dp", "w3Ad", "w3Bp",)), "TD", "w2Dd", ("G2D",),
+    "S01", "w3Dd", "L", "Q", "w3Bd", ("G3ABC",), ("G3D",), "S23", "P",
 )
 
 
 def relay_kernel(
-    x_hbm, q_hbm, g_hbm, pre_hbm, bound_ref, rq_hbm, rf_hbm, cq_hbm, cf_hbm,
+    x_hbm, q_hbm, g_hbm, pre_hbm, bound_hbm, rq_hbm, rf_hbm, cq_hbm, cf_hbm,
     wq_hbm, wf_hbm, mq_hbm, mf_hbm, hq_hbm, hf_hbm, vq_hbm, vf_hbm,
     s_ref, pre_ref, k_ref, weight_ref, moment_ref, rows_ref, cols_ref,
-    xs, gs, go, xt, acc, grad, sacc, norms, roots, col_roots, raw, turn,
+    xs, gs, go, xt, acc, grad, sacc, norms, roots, col_roots, raw, bound, turn,
     own_sem, send_sem, x_sem, g_sem, o_sem, swap_sem,
 ):
     shards, parts, block, span = xs.shape
@@ -249,6 +249,7 @@
                 (q_hbm, raw.at[0]),
                 (g_hbm, raw.at[1]),
                 (pre_hbm, raw.at[2]),
+                (bound_hbm, bound),
                 (rq_hbm, roots.at[0]),
                 (rf_hbm, roots.at[1]),
                 (cq_hbm, col_roots.at[0]),
@@ -264,30 +265,33 @@
             )
         )
     ]
-    for load in loads[:4]:
+    for load in loads[:5]:
         load.start()
-    for load in loads[1:4]:
-        load.wait()
-    sigma_gate = jax.nn.sigmoid(raw[2].astype(f32))
-    cot = to_bf16(
-        raw[1].astype(f32) * (1.0 - bound_ref[...]) * sigma_gate * (1.0 - sigma_gate)
-    )
-
-    @pl.when(pc == 0)
-    def _():
-        gs[fs, py, 0] = raw[0]
-        go[fs] = cot
-
-    @pl.when(pc == 1)
-    def _():
-        gs[fs, py, 1] = cot
-        go[fs] = raw[0]
-
     loads[0].wait()
     pl.semaphore_wait(barrier, 4 + jnp.where(middle, 1, 0))
 
-    for load in loads[4:]:
-        load.start()
+    def cotangents():
+        for load in loads[1:5]:
+            load.wait()
+        sigma_gate = jax.nn.sigmoid(raw[2].astype(f32))
+        cot = to_bf16(
+            raw[1].astype(f32) * (1.0 - bound[...]) * sigma_gate * (1.0 - sigma_gate)
+        )
+
+        @pl.when(pc == 0)
+        def _():
+            gs[fs, py, 0] = raw[0]
+            go[fs] = cot
+
+        @pl.when(pc == 1)
+        def _():
+            gs[fs, py, 1] = cot
+            go[fs] = raw[0]
+
+        for load in loads[5:]:
+            load.start()
+        start(lambda: (go.at[fs], gs.at[fs, py, pc], g_sem.at[0, fs, py]), "core")
+
     half_rows = block // 2
     pending = []
     dones = []
@@ -339,8 +343,6 @@
             start(same, "core")
         if phase == 2 and name != "Ac" and name[1] != "d":
             start(beyond, "core", aside[name[1]])
-
-    start(lambda: (go.at[fs], gs.at[fs, py, pc], g_sem.at[0, fs, py]), "core")
 
     def from_core(label):
         for phase in range(2):
@@ -452,6 +454,8 @@
                 dones.append(swap_norm)
             else:
                 send_outer(step - 1)
+        for load in loads[9:]:
+            load.wait()
         send_outer(features // wide - 1)
 
     def outer_copy(which, step):
@@ -491,6 +495,8 @@
             gradients(int(op[0][1]), op[0][2:], op[1:])
         elif kind in "ow":
             travel(op)
+        elif kind == "C":
+            cotangents()
         elif kind == "T":
             from_core(rest)
             transpose(rest)
@@ -498,7 +504,7 @@
             first, last = int(rest[0]), int(rest[1])
             outer_step(slice(first * width, (last + 1) * width), first == 0, last == 3)
         elif kind == "L":
-            for load in loads[4:8]:
+            for load in loads[5:9]:
                 load.wait()
         elif kind == "P":
             products(pc, slice(2 * width, 3 * width))
@@ -521,8 +527,6 @@
     for step in dones[1:]:
         outer_copy(pc, step).wait_send()
         outer_copy(1 - pc, step).wait_recv()
-    for load in loads[8:]:
-        load.wait()
     for cond, build in pending:
         guarded(cond, lambda build=build: build().wait_send())
 
@@ -551,7 +555,7 @@
             pltpu.VMEM((2, chunk, features), f32),
             pltpu.VMEM((2,) + heads, f32),
         ],
-        in_specs=[hbm] * 4 + [vmem] + [hbm] * 12,
+        in_specs=[hbm] * 17,
         out_specs=[vmem] * 7,
         scratch_shapes=[
             pltpu.VMEM((shards, parts, block, span), bf16),
@@ -565,8 +569,9 @@
             pltpu.VMEM((2, chunk, features), bf16),
             pltpu.VMEM((2,) + heads, bf16),
             pltpu.VMEM((3, block, width), bf16),
+            pltpu.VMEM((1, width), f32),
             pltpu.VMEM((width, features), bf16),
-            pltpu.SemaphoreType.DMA((16,)),
+            pltpu.SemaphoreType.DMA((17,)),
             pltpu.SemaphoreType.DMA((128,)),
             pltpu.SemaphoreType.DMA((2, shards, parts)),
             pltpu.SemaphoreType.DMA((2, shards, 2)),
@@ -577,7 +582,7 @@
             collective_id=0, has_side_effects=True, vmem_limit_bytes=48 * 1024 * 1024
         ),
     )(
-        *in_hbm(x, query_grad, forget_grad, forget_pre), lower_bound.reshape(1, -1), *in_hbm(*held)
+        *in_hbm(x, query_grad, forget_grad, forget_pre, lower_bound.reshape(1, -1), *held)
     )
 
 

time: 58.2 us -> 54.7 us (0.940)
  Pallas kernels: 57.4 us -> 53.9 us
    pallas_call x1, Pallas kernels: 54.3 us -> 50.9 us  [relayed_products(): pl.pallas_call(relay_kernel, out_shape=[pltpu.VMEM((2, chunk, features),...]
where the time goes in v3:
time: 54.7 us; the launch traced here: 54.6 us
  Pallas kernels  53.9 us (99%)
  between operations  0.66 us (1%)
    pallas_call x1, Pallas kernels, relayed_products(): pl.pallas_call(relay_kernel, out_shape=[pltpu.VMEM((2, chunk, features),...  50.9 us
    pallas_call x1, Pallas kernels, finished(): pl.pallas_call(finish_kernel, grid=(steps,), out_shape=flat(f32) + flat(b...  3.03 us

profile of v3, /device:TPU:0, one launch (start us, length us, event | category | flops | bytes accessed | tf_op | source)
XLA Modules:
  0.0 54.6 jit_solution(7970824615986825128)
XLA Ops:
  0.7 50.9 %shard_map.256 = (bf16[2,256,2048]{2,1,0:T(8,128)(2,1)S(1)}, f32[2,256,256]{2,1,0:T(8,128)S(1)}, f32[2,2,128,128]{3,2,1,0:T(8,128)S(1)}, f32[2,256,256]{2,1,0:T(...) custom-call(bf16[128,512]{1,0:T(8,128)(2,1)} %x_hbm.1, ...), custom_call_target="tpu_custom_call" | custom-call | tf_op jit(solution)/shard_map/pallas_call | solution.py:547
  51.5 3.0 %shard_map.257 = (f32[256,256]{1,0:T(8,128)}, f32[256,256]{1,0:T(8,128)}, bf16[256,256]{1,0:T(8,128)(2,1)}, bf16[256,256]{1,0:T(8,128)(2,1)}, f32[256,256]{1,0:T...) custom-call(bf16[2,256,2048]{2,1,0:T(8,128)(2,1)S(1)} %get-tuple-ele, ...), custom_call_target="tpu_custom_call" | custom-call | tf_op jit(solution)/shard_map/pallas_call | solution.py:623

commit v4 on v3

--- a/solution.py
+++ b/solution.py
@@ -163,7 +163,7 @@
     return lax.dot_general(left, right, (dims, ((), ())), preferred_element_type=jnp.float32)
 
 
-LAYERS = "ABCD"
+LAYERS = "ACDB"
 ROUTES = {
     "Ac": ("b", "m", "p", "s"),
     "Bc": ("m", "s"),
@@ -175,14 +175,17 @@
     "Ad": ("b",),
 }
 PROGRAM = (
-    "o0", "o1", "C", "o3", "o2", "w0Bc", "w0Cc", "w1Bc", "w0Ap", "w2Bc", "w0As", "w3Cc", "w1As",
-    "w1Cc", "w1Ap", "w0Dc", "w0Cp", "w0Ad", "w2Ap", "w1Cp", "w1Bs", "w1Cs", "w3Bc", "w2Cc",
-    "w0Cs", "w1Dc", "w2Dc", "w1Cd", "w3Cs", "w2Cp", "w0Bs", "w2Bs", "w0Cd", "w3Cp", "w0Ds",
-    "w2Bp", "w1Ad", "TC", "TA", "w1Bp", "w3Dc", "w2Ad", "w1Dp", "w0Bd", "w1Ds", "w3Bs", "w0Dp",
-    "w0Bp", "w2Cs", "w1Bd", "w3As", "w2As", "TB", "w3Cd", "w3Ap", "w2Dp", "w2Cd", "w2Ds", "w2Bd",
-    ("G2ABC", ("w3Ds",), ("w1Dd",), ("w0Dd", "w3Dp", "w3Ad", "w3Bp",)), "TD", "w2Dd", ("G2D",),
-    "S01", "w3Dd", "L", "Q", "w3Bd", ("G3ABC",), ("G3D",), "S23", "P",
+    "o0", "o1", "C", "o2", "w0Ap", "w1Bc", "o3", "w2Bc", "w0Bc", "w0Cc", "w2Cc", "w0Bp", "w1Cc",
+    "w1Dc", "w1Ap", "w0Cp", "w1As", "w0Dc", "w3Bc", "w2Cp", "w2Ap", "w1Ds", "w1Dp", "w0Cs",
+    "w2Dc", "w0Cd", "w0Bs", "w1Ad", "w1Cp", "w0Ad", "w2Cd", "w0Ds", "w1Bs", "w0Dp", "w2Bp",
+    "w1Bp", "w3Ap", "w1Cs", "w0As", "TA", "w2Dp", "w3Cc", "w2As", "w1Dd", "w3Dc", "w3Bp", "w3Bs",
+    "w2Cs", "w0Dd", "w3Ad", "w2Ds", "w0Bd", "w2Ad", "w1Cd", "w1Bd", "TD", "w2Dd", "TC", "w3Cp",
+    "w2Bs", ("GACD", (), ("w3As", "w3Dp", "w3Bd",)), "TB", "w2Bd",
+    ("GB", (), ("w3Ds", "w3Cs", "w3Cd", "w3Dd",)), "S01", "L", "Q", ("HACD",), ("HB",), "S23",
+    "P",
 )
+
+BLOCKS = {"G": (2, (0, 1, 2), 4), "H": (3, (0, 1), 4)}
 
 
 def relay_kernel(
@@ -363,7 +366,6 @@
                 xt[part * span : (part + 1) * span, lanes] = turned
 
     squares = []
-    tile = features // 4
 
     def own_block(phase, far, label):
         y = 1 - py if far else py
@@ -373,7 +375,8 @@
     def other_block(label):
         return go[pl.ds(2 * layer[label], 2)].reshape(2 * block, width)
 
-    def gradients(phase, labels, events):
+    def gradients(phase, fars, tiles, labels, events):
+        tile = features // tiles
         first, final = labels[0] == LAYERS[0], labels[-1] == LAYERS[-1]
         start_token = LAYERS.index(labels[0]) * 2 * block
         tokens = slice(start_token, start_token + len(labels) * 2 * block)
@@ -388,7 +391,7 @@
 
         def body(step, total):
             rows = pl.ds(pl.multiple_of(step * tile, tile), tile)
-            for far in range(3 if phase == 2 else 2):
+            for far in fars:
                 at = 4 if far == 2 else 2 * (phase - 2) + far
                 right = jnp.concatenate(
                     [other_block(k) if far == 2 else own_block(phase, far, k) for k in labels], axis=0
@@ -436,9 +439,11 @@
             )
         if not final:
 
-            @pl.loop(0, features // wide)
+            broad = 2 * wide
+
+            @pl.loop(0, features // broad)
             def _(step):
-                rows = pl.ds(pl.multiple_of(step * wide, wide), wide)
+                rows = pl.ds(pl.multiple_of(step * broad, broad), broad)
                 product = wide_dot(grad[mine, lanes], grad[rows, lanes], ((1,), (1,)))
                 if not first:
                     product = product + sacc[:, rows]
@@ -492,7 +497,7 @@
     for op in PROGRAM:
         kind, rest = op[0], op[1:]
         if isinstance(op, tuple):
-            gradients(int(op[0][1]), op[0][2:], op[1:])
+            gradients(*BLOCKS[op[0][0]], op[0][1:], op[1:])
         elif kind in "ow":
             travel(op)
         elif kind == "C":
@@ -524,11 +529,11 @@
             k_ref[which, head] = k_ref[which, head] * (
                 (1.0 - stat_decay) / features * scale_twice
             )
+    for cond, build in pending:
+        guarded(cond, lambda build=build: build().wait_send())
     for step in dones[1:]:
         outer_copy(pc, step).wait_send()
         outer_copy(1 - pc, step).wait_recv()
-    for cond, build in pending:
-        guarded(cond, lambda build=build: build().wait_send())
 
 
 def in_hbm(*arrays):

time: 54.7 us -> 53.7 us (0.982)
  Pallas kernels: 53.9 us -> 52.9 us
    pallas_call x1, Pallas kernels: 50.9 us -> 49.9 us  [relayed_products(): pl.pallas_call(relay_kernel, out_shape=[pltpu.VMEM((2, chunk, features),...]
where the time goes in v4:
time: 53.7 us; the launch traced here: 53.6 us
  Pallas kernels  52.9 us (99%)
  between operations  0.66 us (1%)
    pallas_call x1, Pallas kernels, relayed_products(): pl.pallas_call(relay_kernel, out_shape=[pltpu.VMEM((2, chunk, features),...  49.9 us
    pallas_call x1, Pallas kernels, finished(): pl.pallas_call(finish_kernel, grid=(steps,), out_shape=flat(f32) + flat(b...  3.03 us

profile of v4, /device:TPU:0, one launch (start us, length us, event | category | flops | bytes accessed | tf_op | source)
XLA Modules:
  0.0 53.6 jit_solution(6158512606134146995)
XLA Ops:
  0.7 49.9 %shard_map.256 = (bf16[2,256,2048]{2,1,0:T(8,128)(2,1)S(1)}, f32[2,256,256]{2,1,0:T(8,128)S(1)}, f32[2,2,128,128]{3,2,1,0:T(8,128)S(1)}, f32[2,256,256]{2,1,0:T(...) custom-call(bf16[128,512]{1,0:T(8,128)(2,1)} %x_hbm.1, ...), custom_call_target="tpu_custom_call" | custom-call | tf_op jit(solution)/shard_map/pallas_call | solution.py:552
  50.5 3.0 %shard_map.257 = (f32[256,256]{1,0:T(8,128)}, f32[256,256]{1,0:T(8,128)}, bf16[256,256]{1,0:T(8,128)(2,1)}, bf16[256,256]{1,0:T(8,128)(2,1)}, f32[256,256]{1,0:T...) custom-call(bf16[2,256,2048]{2,1,0:T(8,128)(2,1)S(1)} %get-tuple-ele, ...), custom_call_target="tpu_custom_call" | custom-call | tf_op jit(solution)/shard_map/pallas_call | solution.py:628

commit v5 on v4

--- a/solution.py
+++ b/solution.py
@@ -175,14 +175,13 @@
     "Ad": ("b",),
 }
 PROGRAM = (
-    "o0", "o1", "C", "o2", "w0Ap", "w1Bc", "o3", "w2Bc", "w0Bc", "w0Cc", "w2Cc", "w0Bp", "w1Cc",
-    "w1Dc", "w1Ap", "w0Cp", "w1As", "w0Dc", "w3Bc", "w2Cp", "w2Ap", "w1Ds", "w1Dp", "w0Cs",
-    "w2Dc", "w0Cd", "w0Bs", "w1Ad", "w1Cp", "w0Ad", "w2Cd", "w0Ds", "w1Bs", "w0Dp", "w2Bp",
-    "w1Bp", "w3Ap", "w1Cs", "w0As", "TA", "w2Dp", "w3Cc", "w2As", "w1Dd", "w3Dc", "w3Bp", "w3Bs",
-    "w2Cs", "w0Dd", "w3Ad", "w2Ds", "w0Bd", "w2Ad", "w1Cd", "w1Bd", "TD", "w2Dd", "TC", "w3Cp",
-    "w2Bs", ("GACD", (), ("w3As", "w3Dp", "w3Bd",)), "TB", "w2Bd",
-    ("GB", (), ("w3Ds", "w3Cs", "w3Cd", "w3Dd",)), "S01", "L", "Q", ("HACD",), ("HB",), "S23",
-    "P",
+    "o0", "o1", "C", "o2", "w0Ap", "o3", "w1Bc", "w2Bc", "w0Bc", "w2Cc", "w0Cc", "w1Dc", "w1Cc",
+    "w0Bp", "w1Ap", "w1As", "w0Cp", "w3Bc", "w0Dc", "w2Cp", "w1Dp", "w2Ap", "w1Ds", "w0Cs",
+    "w2Dc", "w0Ad", "w0Dp", "w1Bs", "w0Cd", "w1Ad", "w0Bs", "w1Cp", "w2Cd", "w3Ap", "w2As",
+    "w1Bp", "w0As", "w1Cs", "TA", "w2Bp", "w2Dp", "w0Ds", "w3Cc", "w1Dd", "w2Cs", "w3Dc", "w2Ds",
+    "w0Dd", "w3Bp", "w0Bd", "w3Ad", "w1Cd", "w2Ad", "w1Bd", "TD", "TC", "w2Dd", "TB", "w3Cp",
+    "w3Bs", "w3As", ("GACD", (), ("w3Dp",), ("w3Ds", "w2Bs",)), "w3Bd", "w2Bd",
+    ("GB", (), (), ("w3Cs",)), "S01", "w3Cd", "w3Dd", "L", "Q", ("HACD",), ("HB",), "S23", "P",
 )
 
 BLOCKS = {"G": (2, (0, 1, 2), 4), "H": (3, (0, 1), 4)}

time: 53.7 us -> 53.2 us (level)
  no operation moved by 1% of the time
where the time goes in v5:
time: 53.2 us; the launch traced here: 53.1 us
  Pallas kernels  52.4 us (98%)
  between operations  0.66 us (1%)
    pallas_call x1, Pallas kernels, relayed_products(): pl.pallas_call(relay_kernel, out_shape=[pltpu.VMEM((2, chunk, features),...  49.4 us
    pallas_call x1, Pallas kernels, finished(): pl.pallas_call(finish_kernel, grid=(steps,), out_shape=flat(f32) + flat(b...  3.03 us

profile of v5, /device:TPU:0, one launch (start us, length us, event | category | flops | bytes accessed | tf_op | source)
XLA Modules:
  0.0 53.1 jit_solution(17759396322120715609)
XLA Ops:
  0.7 49.4 %shard_map.256 = (bf16[2,256,2048]{2,1,0:T(8,128)(2,1)S(1)}, f32[2,256,256]{2,1,0:T(8,128)S(1)}, f32[2,2,128,128]{3,2,1,0:T(8,128)S(1)}, f32[2,256,256]{2,1,0:T(...) custom-call(bf16[128,512]{1,0:T(8,128)(2,1)} %x_hbm.1, ...), custom_call_target="tpu_custom_call" | custom-call | tf_op jit(solution)/shard_map/pallas_call | solution.py:551
  50.1 3.0 %shard_map.257 = (f32[256,256]{1,0:T(8,128)}, f32[256,256]{1,0:T(8,128)}, bf16[256,256]{1,0:T(8,128)(2,1)}, bf16[256,256]{1,0:T(8,128)(2,1)}, f32[256,256]{1,0:T...) custom-call(bf16[2,256,2048]{2,1,0:T(8,128)(2,1)S(1)} %get-tuple-ele, ...), custom_call_target="tpu_custom_call" | custom-call | tf_op jit(solution)/shard_map/pallas_call | solution.py:627
